TPU v7x, 32 devices: a whole 2x2x4 slice. The times are simulated.
32 devices in a mesh: grp: 2 (over y), kv: 4 (over z), tp: 4 (over x, core).
Axes of the slice: x: 2, y: 2, z: 4, core: 2. Of those that a mesh axis runs over, the one named last changes fastest.
Arguments:
- tokens: bfloat16 [512, 8, 4096], P('kv', 'grp'), parts along dimension 1, may hold values from -72 to 72
- lengths: int32 [8], P('grp'), parts along dimension 0, may hold values from 1 to 512, 768 in all
- chosen: int32 [8, 32, 8, 8], P('grp', 'tp', 'kv'), parts along dimension 0, may hold values from -1 to 7, as said below
- w_query: bfloat16 [4096, 2048], P(None, 'tp'), may hold values from -0.09375 to 0.09375
- w_key: bfloat16 [4096, 2048], P(None, 'tp'), may hold values from -0.09375 to 0.09375
- w_value: bfloat16 [4096, 2048], P(None, 'tp'), may hold values from -0.09375 to 0.09375
- w_gate: bfloat16 [4096, 2, 32], P(None, None, 'tp'), may hold values from -0.09375 to 0.09375
- pool_weights: float32 [2, 32, 64], replicated, may hold values from -1 to 1
- w_out: bfloat16 [2048, 4096], P(None, 'tp'), may hold values from -0.5 to 0.5
Outputs:
- mixed: bfloat16 [512, 8, 4096], P(('kv', 'tp'), 'grp'), parts along dimension 1
There are 2 independent parts, one for each index of `grp`. A program takes and returns all parts, laid end to end along the dimension named above; an argument that names none is the same for every part. Nothing has to cross between parts.
Inputs may be any that keep to these rules, and one draw needn't show every extreme that they name: `chosen`: for query block b the live slots hold min(8, b+1) distinct blocks, all <= b, among them b, b-1 (when b >= 1) and 0; the other slots are -1.
All inputs are finite; a program needn't handle non-finite values.
Results may differ from a plain program's by a relative error of at most 0.014.
Values may be sent and summed in bfloat16 or wider, within the bound.
No kernel may reach another device: no remote copies, remote signals or barrier semaphores. Data moves between devices by JAX's collectives and lax.ppermute only.
A program may use at most 128 MiB of HBM per device.

v0:
```python
from functools import partial

import jax
import jax.numpy as jnp
from jax import lax
from jax.sharding import PartitionSpec as P

HD = 64
QB = 64
L_CMP = 32


LOW_FILL = -1e30


def pooled_blocks(key_rows, pool_weight):
    row_count, seq_count, head_count, head_dim = key_rows.shape
    grouped = key_rows.reshape(row_count // L_CMP, L_CMP, seq_count, head_count, head_dim)
    return (grouped * pool_weight[None, :, None, None, :]).sum(1).astype(jnp.bfloat16)


def pooled_attend(queries, key_pooled, val_pooled, query_pos, lengths):
    head_dim = queries.shape[-1]
    cmp_end = jnp.arange(key_pooled.shape[0]) * L_CMP + L_CMP - 1
    scores = jnp.einsum(
        "qshd,cshd->shqc", queries, key_pooled, preferred_element_type=jnp.float32
    ) * head_dim ** (-0.5)
    usable = (cmp_end[None, None, :] <= query_pos[None, :, None]) & (
        cmp_end[None, None, :] < lengths[:, None, None]
    )
    usable = usable[:, None]
    row_top = jnp.max(jnp.where(usable, scores, LOW_FILL), axis=-1, keepdims=True)
    weights = jnp.where(usable, jnp.exp(scores - row_top), 0.0)
    totals = jnp.sum(weights, axis=-1)
    gathered = jnp.einsum(
        "shqc,cshd->shqd",
        weights.astype(jnp.bfloat16),
        val_pooled,
        preferred_element_type=jnp.float32,
    )
    return gathered / jnp.where(totals > 0, totals, 1.0)[..., None]


def fold_step(running, key_piece, begin_row, queries, chosen, query_pos, lengths):
    maxima, totals, weighted = running
    piece_keys, piece_values = key_piece
    head_dim = queries.shape[-1]
    key_pos = jnp.arange(piece_keys.shape[0])
    key_blk = key_pos // QB
    picked = jnp.any(chosen[..., None] == key_blk, axis=3)
    picked = jnp.repeat(picked, QB, axis=2)
    usable = (
        picked
        & (key_pos[None, None, None, :] <= query_pos[None, None, :, None])
        & (key_pos[None, None, None, :] < lengths[:, None, None, None])
    )
    scores = jnp.einsum(
        "qshd,kshd->shqk", queries, piece_keys, preferred_element_type=jnp.float32
    ) * head_dim ** (-0.5)
    new_max = jnp.maximum(maxima, jnp.max(jnp.where(usable, scores, LOW_FILL), axis=-1))
    weights = jnp.where(usable, jnp.exp(scores - new_max[..., None]), 0.0)
    shrink = jnp.exp(maxima - new_max)
    totals = jnp.sum(weights, axis=-1)
    weighted = jnp.einsum(
        "shqk,kshd->shqd",
        weights.astype(jnp.bfloat16),
        piece_values,
        preferred_element_type=jnp.float32,
    )
    return (new_max, totals, weighted)


def body(tokens, lengths, chosen, w_query, w_key, w_value, w_gate, pool_weights, w_out):
    row_count, seq_count, model_width = tokens.shape
    head_count = w_query.shape[1] // HD
    query_pos = lax.axis_index("kv") * row_count + jnp.arange(row_count)
    flat_rows = tokens.reshape(row_count * seq_count, model_width)

    def project(weight):
        product = jnp.dot(flat_rows, weight, preferred_element_type=jnp.float32)
        return product.astype(jnp.bfloat16).reshape(row_count, seq_count, head_count, HD)

    queries = project(w_query)
    key_rows = project(w_key)
    value_rows = project(w_value)
    gate_values = jax.nn.sigmoid(
        jnp.dot(
            flat_rows,
            w_gate.reshape(model_width, 2 * head_count),
            preferred_element_type=jnp.float32,
        )
    )
    gate_values = gate_values.reshape(row_count, seq_count, 2, head_count)
    key_pooled, val_pooled = (
        lax.all_gather(pooled_blocks(key_rows, pool_weights[0]), "kv", axis=0, tiled=True),
        lax.all_gather(pooled_blocks(value_rows, pool_weights[1]), "kv", axis=0, tiled=True),
    )
    start_state = (
        jnp.full((seq_count, head_count, row_count), LOW_FILL, jnp.float32),
        jnp.zeros((seq_count, head_count, row_count), jnp.float32),
        jnp.zeros((seq_count, head_count, row_count, HD), jnp.float32),
    )
    step_fn = partial(
        fold_step, queries=queries, chosen=chosen, query_pos=query_pos, lengths=lengths
    )
    maxima, totals, weighted = step_fn(
        start_state,
        (
            lax.all_gather(key_rows, "kv", axis=0, tiled=True),
            lax.all_gather(value_rows, "kv", axis=0, tiled=True),
        ),
        jnp.int32(0),
    )
    picked_out = weighted / jnp.where(totals > 0, totals, 1.0)[..., None]
    pooled_out = pooled_attend(queries, key_pooled, val_pooled, query_pos, lengths)
    combined = gate_values[:, :, 0, :, None] * pooled_out.transpose(2, 0, 1, 3) + gate_values[
        :, :, 1, :, None
    ] * picked_out.transpose(2, 0, 1, 3)
    live = query_pos[:, None] < lengths[None, :]
    attended = (
        jnp.where(live[:, :, None, None], combined, 0.0)
        .astype(jnp.bfloat16)
        .reshape(row_count, seq_count, head_count * HD)
    )
    group_count = lax.axis_size("tp")
    all_heads = lax.all_gather(attended, "tp", axis=2, tiled=True)
    group_width = head_count * HD
    col_width = w_out.shape[1]
    grouped_rows = all_heads.reshape(row_count * seq_count, group_count, group_width)
    grouped_weight = w_out.reshape(group_count, group_width, col_width)
    partial_cols = jnp.einsum(
        "rgk,gkc->rgc", grouped_rows, grouped_weight, preferred_element_type=jnp.float32
    )
    column_sum = jnp.sum(partial_cols.astype(jnp.bfloat16).astype(jnp.float32), axis=1)
    column_out = column_sum.astype(jnp.bfloat16).reshape(row_count, seq_count, col_width)
    return lax.all_to_all(column_out, "tp", split_axis=0, concat_axis=2, tiled=True)


def solution(mesh):
    placed = (
        P("kv", "grp", None),
        P("grp"),
        P("grp", "tp", "kv", None),
        P(None, "tp"),
        P(None, "tp"),
        P(None, "tp"),
        P(None, None, "tp"),
        P(),
        P(None, "tp"),
    )
    return jax.shard_map(
        body, mesh=mesh, in_specs=placed, out_specs=P(("kv", "tp"), "grp", None), check_vma=False
    )
```

profile of v0, /device:TPU:21, one launch (start us, length us, event | category | flops | bytes accessed | tf_op | source)
XLA Modules:
  0.0 179.0 jit_solution(17314178159223339070)
XLA Ops:
  6.5 7.0 %reshape.216 = bf16[512,4096]{1,0:T(8,128)(2,1)} reshape(bf16[128,4,4096]{2,1,0:T(4,128)(2,1)} %param.9) | data formatting | bytes 8388608 | tf_op jit(solution)/shard_map/reshape | solution.py:77
  13.5 5.8 %convolution_convert_fusion.1 = bf16[512,512]{1,0:T(8,128)(2,1)S(1)} fusion(bf16[512,4096]{1,0:T(8,128)(2,1)} %reshape.216, bf16[4096,512]{1,0:T(8,128)(2,1)} %param.13), kind=kOutput, calls=%fused_computation.19 | convolution fusion | flops 2147745792 | bytes 8912896 | tf_op jit(solution)/shard_map/dot_general | solution.py:80
  19.8 1.9 %copy.57 = bf16[128,4,8,64]{0,3,2,1:T(8,128)(2,1)} copy(bf16[128,4,8,64]{3,2,1,0:T(8,128)(2,1)S(1)} %reshape.221) | data formatting | bytes 1048576 | tf_op jit(solution)/shard_map/reshape | solution.py:81
  21.8 5.8 %convolution_convert_fusion = bf16[512,512]{1,0:T(8,128)(2,1)S(1)} fusion(bf16[512,4096]{1,0:T(8,128)(2,1)} %reshape.216, bf16[4096,512]{1,0:T(8,128)(2,1)} %param.14), kind=kOutput, calls=%fused_computation.18 | convolution fusion | flops 2147745792 | bytes 8912896 | tf_op jit(solution)/shard_map/dot_general | solution.py:80
  28.1 1.9 %copy.59 = bf16[128,4,8,64]{0,3,2,1:T(8,128)(2,1)} copy(bf16[128,4,8,64]{3,2,1,0:T(8,128)(2,1)S(1)} %reshape.222) | data formatting | bytes 1048576 | tf_op jit(solution)/shard_map/reshape | solution.py:81
  30.3 1.8 %reshape.228 = f32[4,32,4,8,64]{4,3,2,1,0:T(8,128)} reshape(bf16[512,512]{1,0:T(8,128)(2,1)S(1)} %convolution_convert_fusion) | data formatting | bytes 1572864 | tf_op jit(solution)/shard_map/convert_element_type | solution.py:19
  32.6 3.5 %fusion.17 = f32[512,16]{0,1:T(8,128)S(1)} fusion(bf16[512,4096]{1,0:T(8,128)(2,1)} %reshape.216, bf16[4096,2,8]{0,2,1:T(8,128)(2,1)S(1)} %copy-done), kind=kOutput, calls=%fused_computation.30 | convolution fusion | flops 67133440 | bytes 4358144 | tf_op jit(solution)/shard_map/dot_general | solution.py:87
  37.2 5.9 %convolution_convert_fusion.2 = bf16[512,512]{1,0:T(8,128)(2,1)S(1)} fusion(bf16[512,4096]{1,0:T(8,128)(2,1)} %reshape.216, bf16[4096,512]{1,0:T(8,128)(2,1)} %param.12), kind=kOutput, calls=%fused_computation.20 | convolution fusion | flops 2147745792 | bytes 8912896 | tf_op jit(solution)/shard_map/dot_general | solution.py:80
  43.1 1.5 reshape.219
  44.6 2.2 %copy.53 = bf16[128,4,8,64]{0,3,2,1:T(8,128)(2,1)S(1)} copy(bf16[128,4,8,64]{3,2,1,0:T(8,128)(2,1)} %reshape.219) | data formatting | bytes 1048576 | tf_op jit(solution)/shard_map/reshape | solution.py:81
  46.8 1.9 %multiply_reduce_fusion = bf16[4,4,8,64]{3,2,1,0:T(8,128)(2,1)S(1)} fusion(f32[4,32,4,8,64]{4,3,2,1,0:T(8,128)} %reshape.228, f32[32,64]{1,0:T(8,128)S(1)} %get-tuple-element.9), kind=kLoop, calls=%fused_computation.9 | loop fusion | flops 516096 | bytes 1073152 | tf_op jit(solution)/shard_map/reduce_sum | solution.py:19
  48.7 14.4 %all_gather.16 = bf16[16,4,8,64]{3,2,1,0:T(8,128)(2,1)S(1)} all-gather(bf16[4,4,8,64]{3,2,1,0:T(8,128)(2,1)S(1)} %multiply_reduce_fusion), channel_id=1, replica_groups=mesh['grp'=2,'kv'=4,'tp'=4] {'kv'}, dimensions={0}, use_global_device_ids=true | all-gather | bytes 81920 | tf_op jit(solution)/shard_map/all_gather | solution.py:96
  63.4 10.8 %all_gather.15 = bf16[16,4,8,64]{3,2,1,0:T(8,128)(2,1)S(1)} all-gather(bf16[4,4,8,64]{3,2,1,0:T(8,128)(2,1)S(1)} %multiply_reduce_fusion.1), channel_id=1, replica_groups=mesh['grp'=2,'kv'=4,'tp'=4] {'kv'}, dimensions={0}, use_global_device_ids=true | all-gather | bytes 81920 | tf_op jit(solution)/shard_map/all_gather | solution.py:95
  75.7 4.3 %select_reduce_fusion = (f32[4,8,128]{2,1,0:T(8,128)S(1)}, f32[4,8,128,512]{3,2,1,0:T(8,128)S(1)}) fusion(pred[4,512]{1,0:T(4,128)(4,1)S(1)} %iota_compare_fusion.1, pred[128,512]{1,0:T(8,128)(4,1)S(1)} %iota_compare_fusion, pred[4,8,2,512]{3,2,1,0:T(4,128)(4,1)S(1)} %compare_reduce_fusion, bf16[128,4,8,64]{0,3,2,1:T(8,128)(2,1)S(1)} %copy.53, ...), kind=kOutput, calls=%fused_computation.2 | convolution fusion | flops 278917120 | bytes 11126784 | tf_op jit(solution)/shard_map/qshd,kshd->shqk/dot_general | solution.py:57
  79.9 4.5 %fusion.2 = (f32[4,8,128]{2,1,0:T(8,128)S(1)}, bf16[4,8,128,512]{3,2,1,0:T(8,128)(2,1)}) fusion(f32[4,8,128,512]{3,2,1,0:T(8,128)S(1)} %get-tuple-element.12, f32[4,8,128]{2,1,0:T(8,128)S(1)} %broadcast_maximum_fusion, pred[4,512]{1,0:T(4,128)(4,1)S(1)} %iota_compare_fusion.1, pred[128,512]{1,0:T(8,128)(4,1)S(1)} %iota_compare_fusion, ...), kind=kLoop, calls=%fused_computation.5 | loop fusion | flops 14675968 | bytes 12716032 | tf_op jit(solution)/shard_map/reduce_sum | solution.py:63
  84.4 31.2 %all-gather.6.cloned.1.call-done = bf16[512,4,8,64]{0,3,2,1:T(8,128)(2,1)} async-done(((bf16[128,4,8,64]{0,3,2,1:T(8,128)(2,1)}), bf16[512,4,8,64]{0,3,2,1:T(8,128)(2,1)}) %all-gather.6.cloned.1.call-update) | async-done | bytes 2097168 | tf_op jit(solution)/shard_map/all_gather | solution.py:110
  115.7 4.4 %fusion.11 = f32[128,4,8,64]{0,3,2,1:T(8,128)S(1)} fusion(bf16[4,8,128,512]{3,2,1,0:T(8,128)(2,1)} %get-tuple-element.6, bf16[512,4,8,64]{0,3,2,1:T(8,128)(2,1)} %all-gather.6.cloned.1.call-done, f32[128,4,8]{0,2,1:T(8,128)S(1)} %compare_select_fusion, f32[128,4,8]{0,2,1:T(8,128)S(1)} %copy.56), kind=kOutput, calls=%fused_computation.22 | convolution fusion | flops 268959744 | bytes 7372800 | tf_op jit(solution)/shard_map/shqk,kshd->shqd/dot_general | solution.py:64
  120.5 1.2 copy.60
  121.7 23.7 %all-gather.8.cloned.1.call-done = bf16[128,4,2048]{2,1,0:T(4,128)(2,1)} async-done(((bf16[128,4,512]{2,1,0:T(4,128)(2,1)}), bf16[128,4,2048]{2,1,0:T(4,128)(2,1)}) %all-gather.8.cloned.1.call-update) | async-done | bytes 2097168 | tf_op jit(solution)/shard_map/all_gather | solution.py:126
  145.4 3.1 %reshape.224 = bf16[512,4,512]{2,1,0:T(4,128)(2,1)S(1)} reshape(bf16[128,4,2048]{2,1,0:T(4,128)(2,1)} %all-gather.8.cloned.1.call-done) | data formatting | bytes 4194304 | tf_op jit(solution)/shard_map/reshape | solution.py:129
  148.6 4.6 %convert_reduce_fusion = bf16[512,1024]{1,0:T(8,128)(2,1)S(1)} fusion(bf16[4,512,1024]{2,1,0:T(8,128)(2,1)} %bitcast.66, bf16[512,4,512]{2,1,0:T(4,128)(2,1)S(1)} %reshape.224), kind=kOutput, calls=%fused_computation.7 | convolution fusion | flops 2151153664 | bytes 7340032 | tf_op jit(solution)/shard_map/rgk,gkc->rgc/dot_general | solution.py:131
  153.7 16.1 %all_to_all.18 = bf16[128,4,1024]{2,1,0:T(4,128)(2,1)S(1)} all-to-all(bf16[128,4,1024]{2,1,0:T(4,128)(2,1)S(1)} %reshape.226), channel_id=1, replica_groups=mesh['grp'=2,'kv'=4,'tp'=4] {'tp'}, dimensions={0} | all-to-all | bytes 2097152 | tf_op jit(solution)/shard_map/all_to_all | solution.py:136
  170.1 0.8 copy.65
  170.9 1.6 reshape.229
  (45 shorter events, 5.7 us)
Async XLA Ops:
  6.5 26.1 %copy-start = (bf16[4096,2,8]{0,2,1:T(8,128)(2,1)S(1)}, bf16[4096,2,8]{0,2,1:T(8,128)(2,1)}, u32[]{:S(2)}) copy-start(bf16[4096,2,8]{0,2,1:T(8,128)(2,1)} %param.15) | copy-start | bytes 393220
  6.5 69.1 %all-gather.4.cloned.1.call-start = ((), (), s32[]{:S(2)}) async-start(), calls=%async_computation.1 | async-start | bytes 2621440 | tf_op jit(solution)/shard_map/all_gather | solution.py:109
  21.7 93.9 %all-gather.6.cloned.1.call-start = ((), (), s32[]{:S(2)}) async-start(), calls=%async_computation.2 | async-start | bytes 2621440 | tf_op jit(solution)/shard_map/all_gather | solution.py:110
  27.6 5.0 %copy-start.3 = (f32[2,32,64]{2,1,0:T(8,128)S(1)}, f32[2,32,64]{2,1,0:T(8,128)}, u32[]{:S(2)}) copy-start(f32[2,32,64]{2,1,0:T(8,128)} %param.16) | copy-start | bytes 49156
  30.1 115.3 %all-gather.8.cloned.1.call-start = ((), (), s32[]{:S(2)}) async-start(), calls=%async_computation.3 | async-start | bytes 2621440 | tf_op jit(solution)/shard_map/all_gather | solution.py:126
  43.0 31.2 %copy-start.2 = (s32[4,8,2,8]{3,2,1,0:T(2,128)S(1)}, s32[4,8,2,8]{3,2,1,0:T(2,128)}, u32[]{:S(2)}) copy-start(s32[4,8,2,8]{3,2,1,0:T(2,128)} %param.11) | copy-start | bytes 6148
  43.0 31.7 %copy-start.4 = (s32[4]{0:T(128)S(1)}, s32[4]{0:T(128)}, u32[]{:S(2)}) copy-start(s32[4]{0:T(128)} %param.10) | copy-start | bytes 52
  153.2 19.3 %copy-start.1 = (bf16[4096,2,8]{0,2,1:T(8,128)(2,1)S(1)}, bf16[4096,2,8]{0,2,1:T(8,128)(2,1)}, u32[]{:S(2)}) copy-start(bf16[4096,2,8]{0,2,1:T(8,128)(2,1)} %param.15) | copy-start | bytes 393220
Sparse Core Ops, SparseCore 0:
  21.9 47.7 all-gather.3
  71.2 44.4 all-gather.5
  121.8 23.5 all-gather.7
where the time goes:
time: 182 us; the launch traced here: 179 us
  waiting for transfers between devices  55 us (30%)
  blocking collectives  41.3 us (23%)
  matrix products  34.9 us (19%)
  local copies, waits for them, and re-layouts  26.4 us (15%)
  between operations  13.4 us (7%)
  other arithmetic  7.74 us (4%)
    all_gather x1, waiting for transfers between devices, body(): lax.all_gather(value_rows, 'kv', axis=0, tiled=True)  31.2 us
    all_gather x1, waiting for transfers between devices, body(): all_heads = lax.all_gather(attended, 'tp', axis=2, tiled=True)  23.7 us
    dot_general x3, matrix products, project(): product = jnp.dot(flat_rows, weight, preferred_element_type=jnp.float32)  17.4 us
    all_to_all x1, blocking collectives, body(): lax.all_to_all(column_out, 'tp', split_axis=0, concat_axis=2, tiled=True)  16.1 us
    all_gather x1, blocking collectives, body(): lax.all_gather(pooled_blocks(value_rows, pool_weights[1]), 'kv', axis=0,...  14.4 us
    all_gather x1, blocking collectives, body(): lax.all_gather(pooled_blocks(key_rows, pool_weights[0]), 'kv', axis=0, ti...  10.8 us
    reshape x6, local copies, waits for them, and re-layouts, project(): product.astype(jnp.bfloat16).reshape(row_count, seq_count, head_count, HD)  8.64 us
    reshape x1, local copies, waits for them, and re-layouts, body(): flat_rows = tokens.reshape(row_count * seq_count, model_width)  6.95 us
  transfers between devices with their start and end apart: 3, of which 2 were waited for; matrix products, arithmetic and copies ran while one was open for 21% of the time, Pallas kernels for 0%

commit v1 on v0

--- a/solution.py
+++ b/solution.py
@@ -3,6 +3,8 @@
 import jax
 import jax.numpy as jnp
 from jax import lax
+from jax.experimental import pallas as pl
+from jax.experimental.pallas import tpu as pltpu
 from jax.sharding import PartitionSpec as P
 
 HD = 64
@@ -70,7 +72,7 @@
     return (new_max, totals, weighted)
 
 
-def body(tokens, lengths, chosen, w_query, w_key, w_value, w_gate, pool_weights, w_out):
+def general_body(tokens, lengths, chosen, w_query, w_key, w_value, w_gate, pool_weights, w_out):
     row_count, seq_count, model_width = tokens.shape
     head_count = w_query.shape[1] // HD
     query_pos = lax.axis_index("kv") * row_count + jnp.arange(row_count)
@@ -134,6 +136,302 @@
     column_sum = jnp.sum(partial_cols.astype(jnp.bfloat16).astype(jnp.float32), axis=1)
     column_out = column_sum.astype(jnp.bfloat16).reshape(row_count, seq_count, col_width)
     return lax.all_to_all(column_out, "tp", split_axis=0, concat_axis=2, tiled=True)
+
+
+def length_ranks(len_ref, seq_count):
+    lens = [len_ref[s] for s in range(seq_count)]
+    ranks = []
+    for s in range(seq_count):
+        rank = jnp.int32(0)
+        for other in range(seq_count):
+            if other != s:
+                ahead = lens[other] >= lens[s] if other < s else lens[other] > lens[s]
+                rank = rank + ahead.astype(jnp.int32)
+        ranks.append(rank)
+    return lens, ranks
+
+
+def sort_rows(len_ref, x_ref, rows_ref):
+    row_count, seq_count, _ = x_ref.shape
+    _, ranks = length_ranks(len_ref, seq_count)
+    for s in range(seq_count):
+        start = pl.multiple_of(ranks[s] * row_count, row_count)
+        rows_ref[pl.ds(start, row_count), :] = x_ref[:, s, :]
+
+
+def dot32(a, b):
+    return jnp.dot(a, b, preferred_element_type=jnp.float32)
+
+
+def dot_nt(a, b):
+    return lax.dot_general(a, b, (((1,), (1,)), ((), ())), preferred_element_type=jnp.float32)
+
+
+def kv_kernel(len_ref, x_ref, wk_ref, wv_ref, long_ref, short_ref, rows_ref):
+    step = pl.program_id(0)
+    half = pl.num_programs(0) // 2
+
+    @pl.when(step == 0)
+    def _():
+        sort_rows(len_ref, x_ref, rows_ref)
+
+    def emit(w_ref):
+        out = dot32(rows_ref[...], w_ref[...]).astype(jnp.bfloat16)
+        out = out.reshape((2,) + long_ref.shape[:2] + out.shape[1:])
+        long_ref[...] = out[0]
+        short_ref[...] = out[1]
+
+    @pl.when(step < half)
+    def _():
+        emit(wk_ref)
+
+    @pl.when(step >= half)
+    def _():
+        emit(wv_ref)
+
+
+def q_kernel(len_ref, x_ref, wq_ref, wg_ref, q_ref, gate_ref, rows_ref):
+    step = pl.program_id(0)
+
+    @pl.when(step == 0)
+    def _():
+        sort_rows(len_ref, x_ref, rows_ref)
+        gate_ref[...] = jax.nn.sigmoid(dot_nt(rows_ref[...], wg_ref[...]))
+
+    q_ref[...] = dot32(rows_ref[...], wq_ref[...]).astype(jnp.bfloat16)
+
+
+def attend_kernel(len_ref, pos_ref, q_ref, gate_ref, long_ref, short_ref, a_ref, b_ref, c_ref, d_ref, pool_ref, out_ref):
+    seq_count, row_count, width = q_ref.shape
+    head_count = width // HD
+    lens, ranks = length_ranks(len_ref, seq_count)
+    block = pos_ref[0]
+    scale = HD ** -0.5
+    per_block = row_count // L_CMP
+    row_id = lax.broadcasted_iota(jnp.int32, (row_count, 1), 0)
+    tri = lax.broadcasted_iota(jnp.int32, (row_count, row_count), 1) <= row_id
+    cmp_end = lax.broadcasted_iota(jnp.int32, (row_count, per_block), 1) * L_CMP + L_CMP - 1
+    cmp_tri = cmp_end <= row_id
+    pool_rows = [
+        jnp.concatenate([pool_ref[i]] * head_count, axis=1) for i in range(2)
+    ]
+
+    def pooled(rows, weight):
+        grouped = rows.astype(jnp.float32).reshape(per_block, L_CMP, width)
+        return (grouped * weight[None]).sum(1)
+
+    for r in range(seq_count):
+        length = jnp.int32(0)
+        for s in range(seq_count):
+            length = length + jnp.where(ranks[s] == r, lens[s], 0)
+        live = block * row_count + row_id < length
+        if r == 0:
+            pieces = [long_ref[0], a_ref[0], c_ref[0], d_ref[0]]
+        elif r == 1:
+            pieces = [long_ref[1], a_ref[1], c_ref[1]]
+        else:
+            pieces = [short_ref[r - 2], b_ref[r - 2]]
+        keys = jnp.concatenate([p[:, :width] for p in pieces], axis=0)
+        vals = jnp.concatenate([p[:, width:] for p in pieces], axis=0)
+        key_pool = jnp.concatenate([pooled(p[:, :width], pool_rows[0]) for p in pieces], axis=0).astype(jnp.bfloat16)
+        val_pool = jnp.concatenate([pooled(p[:, width:], pool_rows[1]) for p in pieces], axis=0).astype(jnp.bfloat16)
+        usable = jnp.concatenate(
+            [tri] + [jnp.full((row_count, row_count), block >= i) for i in range(1, len(pieces))], axis=1
+        )
+        cmp_id = lax.broadcasted_iota(jnp.int32, (row_count, per_block * len(pieces)), 1)
+        cmp_blk = cmp_id // per_block
+        cmp_usable = ((cmp_blk == 0) & (cmp_id * L_CMP + L_CMP - 1 <= row_id)) | (
+            (cmp_blk > 0) & (cmp_blk <= block)
+        )
+
+        def soft(query, key, value, mask):
+            scores = jnp.where(mask, dot_nt(query, key) * scale, LOW_FILL)
+            top = jnp.max(scores, axis=1, keepdims=True)
+            weights = jnp.where(mask, jnp.exp(scores - top), 0.0)
+            total = jnp.sum(weights, axis=1, keepdims=True)
+            return dot32(weights.astype(jnp.bfloat16), value) / jnp.where(total > 0, total, 1.0)
+
+        outs = []
+        for h in range(head_count):
+            cols = slice(h * HD, (h + 1) * HD)
+            query = q_ref[r][:, cols]
+            picked = soft(query, keys[:, cols], vals[:, cols], usable)
+            pool = soft(query, key_pool[:, cols], val_pool[:, cols], cmp_usable)
+            mixed = gate_ref[r][:, h : h + 1] * pool + gate_ref[r][:, head_count + h : head_count + h + 1] * picked
+            outs.append(jnp.where(live, mixed, 0.0))
+        out_ref[r] = jnp.concatenate(outs, axis=1).astype(jnp.bfloat16)
+
+
+def part_product(rows_ref, w_ref):
+    return dot32(rows_ref[...], w_ref[0]).astype(jnp.bfloat16).astype(jnp.float32)
+
+
+def near_kernel(idx_ref, a_ref, b_ref, wa_ref, wb_ref, out_ref):
+    out_ref[...] = part_product(a_ref, wa_ref) + part_product(b_ref, wb_ref)
+
+
+def far_kernel(idx_ref, a_ref, b_ref, wa_ref, wb_ref, near_ref, *out_refs):
+    total = near_ref[...] + (part_product(a_ref, wa_ref) + part_product(b_ref, wb_ref))
+    seq_count, row_count, width = out_refs[-1].shape
+    out_refs[-1][...] = total.astype(jnp.bfloat16).reshape(out_refs[-1].shape)
+    piece = out_refs[0].shape[1]
+    for k in range(len(out_refs) - 1):
+        start = pl.multiple_of(idx_ref[k] * piece, piece)
+        out_refs[k][...] = out_refs[-1][:, pl.ds(start, piece), :]
+
+
+def live_body(tokens, lengths, chosen, w_query, w_key, w_value, w_gate, pool_weights, w_out):
+    row_count, seq_count, model_width = tokens.shape
+    width = w_query.shape[1]
+    head_count = width // HD
+    flat = row_count * seq_count
+    kv_at = lax.axis_index("kv").astype(jnp.int32)
+    tp_at = lax.axis_index("tp").astype(jnp.int32)
+    tp_size = lax.axis_size("tp")
+    half = width // 2
+    two = seq_count // 2
+    bf16 = jnp.bfloat16
+    params = pltpu.CompilerParams(vmem_limit_bytes=56 * 2**20, dimension_semantics=("arbitrary",))
+    whole = lambda shape: pl.BlockSpec(shape, lambda *_: (0,) * len(shape))
+
+    kv_long, kv_short = pl.pallas_call(
+        kv_kernel,
+        grid_spec=pltpu.PrefetchScalarGridSpec(
+            num_scalar_prefetch=1,
+            grid=(4,),
+            in_specs=[
+                pl.BlockSpec(tokens.shape, lambda i, n: (0, 0, 0), pipeline_mode=pl.Buffered(1)),
+                pl.BlockSpec((model_width, half), lambda i, n: (0, jnp.minimum(i, 1))),
+                pl.BlockSpec((model_width, half), lambda i, n: (0, jnp.maximum(i - 2, 0))),
+            ],
+            out_specs=[pl.BlockSpec((two, row_count, half), lambda i, n: (0, 0, i))] * 2,
+            scratch_shapes=[pltpu.VMEM((flat, model_width), bf16)],
+        ),
+        out_shape=[jax.ShapeDtypeStruct((two, row_count, 2 * width), bf16)] * 2,
+        compiler_params=params,
+        name="kv_rows",
+    )(lengths, tokens, w_key, w_value)
+
+    got_a = lax.ppermute(kv_long, "kv", [(0, 1), (1, 2), (2, 3)])
+    got_b = lax.ppermute(kv_short, "kv", [(0, 1)])
+    got_c = lax.ppermute(got_a, "kv", [(1, 2), (2, 3)])
+    got_d = lax.ppermute(got_c[:1], "kv", [(2, 3)])
+
+    gate_rows = w_gate.transpose(1, 2, 0).reshape(2 * head_count, model_width)
+    queries, gates = pl.pallas_call(
+        q_kernel,
+        grid_spec=pltpu.PrefetchScalarGridSpec(
+            num_scalar_prefetch=1,
+            grid=(2,),
+            in_specs=[
+                pl.BlockSpec(tokens.shape, lambda i, n: (0, 0, 0), pipeline_mode=pl.Buffered(1)),
+                pl.BlockSpec((model_width, half), lambda i, n: (0, i)),
+                whole(gate_rows.shape),
+            ],
+            out_specs=[
+                pl.BlockSpec((flat, half), lambda i, n: (0, i)),
+                whole((flat, 2 * head_count)),
+            ],
+            scratch_shapes=[pltpu.VMEM((flat, model_width), bf16)],
+        ),
+        out_shape=[
+            jax.ShapeDtypeStruct((flat, width), bf16),
+            jax.ShapeDtypeStruct((flat, 2 * head_count), jnp.float32),
+        ],
+        compiler_params=params,
+        name="query_rows",
+    )(lengths, tokens, w_query, gate_rows)
+    queries = queries.reshape(seq_count, row_count, width)
+    gates = gates.reshape(seq_count, row_count, 2 * head_count)
+
+    operands = (queries, gates, kv_long, kv_short, got_a, got_b, got_c, got_d, pool_weights)
+    attended = pl.pallas_call(
+        attend_kernel,
+        grid_spec=pltpu.PrefetchScalarGridSpec(
+            num_scalar_prefetch=2,
+            grid=(1,),
+            in_specs=[whole(o.shape) for o in operands],
+            out_specs=whole(queries.shape),
+        ),
+        out_shape=jax.ShapeDtypeStruct(queries.shape, bf16),
+        compiler_params=params,
+        name="attend",
+    )(lengths, kv_at[None], *operands)
+
+    attended = attended.reshape(flat, width)
+    swap = lambda x, bit: lax.ppermute(x, "tp", [(t, t ^ bit) for t in range(tp_size)])
+    far_a = swap(attended, 2)
+    near_b = swap(attended, 1)
+    far_b = swap(far_a, 1)
+    order = jnp.stack([tp_at, tp_at ^ 1, tp_at ^ 2, tp_at ^ 3])
+    col_width = w_out.shape[1]
+    weight = w_out.reshape(tp_size, width, col_width)
+
+    def weight_spec(k):
+        return pl.BlockSpec((1, width, col_width), lambda i, n: (n[k], 0, 0))
+
+    near = pl.pallas_call(
+        near_kernel,
+        grid_spec=pltpu.PrefetchScalarGridSpec(
+            num_scalar_prefetch=1,
+            grid=(1,),
+            in_specs=[whole((flat, width))] * 2 + [weight_spec(0), weight_spec(1)],
+            out_specs=whole((flat, col_width)),
+        ),
+        out_shape=jax.ShapeDtypeStruct((flat, col_width), jnp.float32),
+        compiler_params=params,
+        name="near_heads",
+    )(order, attended, near_b, weight, weight)
+    piece = row_count // tp_size
+    parts = pl.pallas_call(
+        far_kernel,
+        grid_spec=pltpu.PrefetchScalarGridSpec(
+            num_scalar_prefetch=1,
+            grid=(1,),
+            in_specs=[whole((flat, width))] * 2 + [weight_spec(2), weight_spec(3), whole((flat, col_width))],
+            out_specs=[whole((seq_count, piece, col_width))] * tp_size,
+            scratch_shapes=[pltpu.VMEM((seq_count, row_count, col_width), bf16)],
+        ),
+        out_shape=[jax.ShapeDtypeStruct((seq_count, piece, col_width), bf16)] * tp_size,
+        compiler_params=params,
+        name="far_heads",
+    )(order, far_a, far_b, weight, weight, near)
+    got = [parts[0]] + [swap(parts[k], k) for k in (2, 3, 1)]
+    got = [got[0], got[3], got[1], got[2]]
+    return pl.pallas_call(
+        place_kernel,
+        grid_spec=pltpu.PrefetchScalarGridSpec(
+            num_scalar_prefetch=2,
+            grid=(1,),
+            in_specs=[whole((seq_count, piece, col_width))] * tp_size,
+            out_specs=whole((piece, seq_count, tp_size * col_width)),
+        ),
+        out_shape=jax.ShapeDtypeStruct((piece, seq_count, tp_size * col_width), bf16),
+        compiler_params=params,
+        name="place",
+    )(lengths, order, *got)
+
+
+def place_kernel(len_ref, idx_ref, *refs):
+    out_ref = refs[-1]
+    seq_count, piece, col_width = refs[0].shape
+    _, ranks = length_ranks(len_ref, seq_count)
+    for k, part in enumerate(refs[:-1]):
+        start = pl.multiple_of(idx_ref[k] * col_width, col_width)
+        for s in range(seq_count):
+            out_ref[:, s, pl.ds(start, col_width)] = part[ranks[s]]
+
+
+def body(tokens, lengths, chosen, *weights):
+    row_count, seq_count, _ = tokens.shape
+    kv_size = lax.axis_size("kv")
+    seq_len = row_count * kv_size
+    live_total = seq_count * seq_len * 3 // 8
+    most = [live_total // (row_count * j + 1) for j in range(1, kv_size)]
+    dense = seq_len // QB <= chosen.shape[-1]
+    if dense and kv_size == 4 and seq_count == 4 and lax.axis_size("tp") == 4 and most[1] <= 2 and most[2] <= 1:
+        return live_body(tokens, lengths, chosen, *weights)
+    return general_body(tokens, lengths, chosen, *weights)
 
 
 def solution(mesh):

time: 182 us -> 129 us (0.71); the launches traced: 179 us -> 129 us
  Pallas kernels: 0 us -> 64.3 us
  blocking collectives: 41.3 us -> 0 us
  matrix products: 34.9 us -> 0 us
  local copies, waits for them, and re-layouts: 26.4 us -> 3.17 us
  starting transfers between devices: 0.27 us -> 20.3 us
  waiting for transfers between devices: 55 us -> 40.3 us
  between operations: 13.4 us -> 0.1 us
  other arithmetic: 7.74 us -> 0.64 us
    pallas_call x0 -> x6, Pallas kernels: none -> 64.3 us  [the longest x1 18.4 us: live_body(): pl.pallas_call(attend_kernel, grid_spec=pltpu.PrefetchScalarGridSpec(num_...]
    all_gather x3 -> x0, waiting for transfers between devices: 55 us -> none  [the longest x1 31.2 us: body(): lax.all_gather(value_rows, 'kv', axis=0, tiled=True)]
    ppermute x0 -> x10, waiting for transfers between devices: none -> 40.3 us  [the longest x6 18.7 us: live_body(): lax.ppermute(x, 'tp', [(t, t ^ bit) for t in range(tp_size)])]
    dot_general x9 -> x0, matrix products: 34.9 us -> none  [the longest x3 17.4 us: project(): product = jnp.dot(flat_rows, weight, preferred_element_type=jnp.float32)]
    all_gather x2 -> x0, blocking collectives: 25.3 us -> none  [the longest x1 14.4 us: body(): lax.all_gather(pooled_blocks(value_rows, pool_weights[1]), 'kv', axis=0,...]
    reshape x11 -> x0, local copies, waits for them, and re-layouts: 20.7 us -> none  [the longest x6 8.64 us: project(): product.astype(jnp.bfloat16).reshape(row_count, seq_count, head_count, HD)]
    ppermute x0 -> x10, starting transfers between devices: none -> 20.3 us  [the longest x6 9.83 us: live_body(): lax.ppermute(x, 'tp', [(t, t ^ bit) for t in range(tp_size)])]
    all_to_all x1 -> x0, blocking collectives: 16.1 us -> none  [body(): lax.all_to_all(column_out, 'tp', split_axis=0, concat_axis=2, tiled=True)]
  transfers between devices with their start and end apart: 3 -> 10, of which waited for: 2 -> 5; matrix products, arithmetic and copies ran while one was open for 21% -> 1% of each run, Pallas kernels for 0% -> 15%
where the time goes in v1:
time: 129 us
  Pallas kernels  64.3 us (50%)
  waiting for transfers between devices  40.3 us (31%)
  starting transfers between devices  20.3 us (16%)
  local copies, waits for them, and re-layouts  3.17 us (2%)
    ppermute x6, waiting for transfers between devices, live_body(): lax.ppermute(x, 'tp', [(t, t ^ bit) for t in range(tp_size)])  18.7 us
    pallas_call x1, Pallas kernels, live_body(): pl.pallas_call(attend_kernel, grid_spec=pltpu.PrefetchScalarGridSpec(num_...  18.4 us
    pallas_call x1, Pallas kernels, live_body(): pl.pallas_call(kv_kernel, grid_spec=pltpu.PrefetchScalarGridSpec(num_scal...  18.2 us
    pallas_call x1, Pallas kernels, live_body(): pl.pallas_call(q_kernel, grid_spec=pltpu.PrefetchScalarGridSpec(num_scala...  13.6 us
    ppermute x1, waiting for transfers between devices, live_body(): got_a = lax.ppermute(kv_long, 'kv', [(0, 1), (1, 2), (2, 3)])  11.7 us
    ppermute x1, waiting for transfers between devices, live_body(): got_c = lax.ppermute(got_a, 'kv', [(1, 2), (2, 3)])  9.93 us
    ppermute x6, starting transfers between devices, live_body(): lax.ppermute(x, 'tp', [(t, t ^ bit) for t in range(tp_size)])  9.83 us
    pallas_call x1, Pallas kernels, live_body(): pl.pallas_call(far_kernel, grid_spec=pltpu.PrefetchScalarGridSpec(num_sca...  5.54 us
  transfers between devices with their start and end apart: 10, of which 5 were waited for; matrix products, arithmetic and copies ran while one was open for 1% of the time, Pallas kernels for 15%

profile of v1, /device:TPU:21, one launch (start us, length us, event | category | flops | bytes accessed | tf_op | source)
XLA Modules:
  0.0 128.8 jit_solution(15426988769929666876)
XLA Ops:
  0.0 18.2 %kv_rows.1 = (bf16[2,128,1024]{2,1,0:T(8,128)(2,1)}, bf16[2,128,1024]{2,1,0:T(8,128)(2,1)}) custom-call(s32[4]{0:T(128)} %len_ref.7, bf16[128,4,4096]{2,1,0:T(4,128)(2,1)} %x_ref.3, bf16[4096,512]{1,0:T(8,128)(2,1)} %wk_ref.1, bf16[4096,512]{1,0:T(8,128)(2,1)} %wv_ref.1), custom_call_target="tpu_custom_call" | custom-call | tf_op jit(solution)/shard_map/kv_rows/pallas_call | solution.py:297
  18.2 3.2 %collective-permute-start = (bf16[2,128,1024]{2,1,0:T(8,128)(2,1)}, bf16[2,128,1024]{2,1,0:T(8,128)(2,1)S(1)}, u32[]{:S(2)}, u32[]{:S(2)}) collective-permute-start(bf16[2,128,1024]{2,1,0:T(8,128)(2,1)} %get-tuple-element.15.long_ref), channel_id=1, source_target_pairs={{0,4},{4,8},{8,12},{1,5},{5,9},{9,13},{2,6},{6,10},{10,14},{3,7},{... | collective-permute-start | bytes 1572872 | tf_op jit(solution)/shard_map/ppermute | solution.py:315
  21.4 11.7 %collective-permute-done.a_ref = bf16[2,128,1024]{2,1,0:T(8,128)(2,1)S(1)} collective-permute-done((bf16[2,128,1024]{2,1,0:T(8,128)(2,1)}, bf16[2,128,1024]{2,1,0:T(8,128)(2,1)S(1)}, u32[]{:S(2)}, u32[]{:S(2)}) %collective-permute-start) | collective-permute-done | bytes 524320 | tf_op jit(solution)/shard_map/ppermute | solution.py:315
  33.1 3.2 %collective-permute-start.2 = (bf16[2,128,1024]{2,1,0:T(8,128)(2,1)S(1)}, bf16[2,128,1024]{2,1,0:T(8,128)(2,1)S(1)}, u32[]{:S(2)}, u32[]{:S(2)}) collective-permute-start(bf16[2,128,1024]{2,1,0:T(8,128)(2,1)S(1)} %collective-permute-done.a_ref), channel_id=1, source_target_pairs={{4,8},{8,12},{5,9},{9,13},{6,10},{10,14},{7,11},{11,15},{20,24},{2... | collective-permute-start | bytes 1572872 | tf_op jit(solution)/shard_map/ppermute | solution.py:317
  36.3 0.7 collective-permute-start.1
  37.0 9.9 %collective-permute-done.2.c_ref = bf16[2,128,1024]{2,1,0:T(8,128)(2,1)S(1)} collective-permute-done((bf16[2,128,1024]{2,1,0:T(8,128)(2,1)S(1)}, bf16[2,128,1024]{2,1,0:T(8,128)(2,1)S(1)}, u32[]{:S(2)}, u32[]{:S(2)}) %collective-permute-start.2) | collective-permute-done | bytes 524320 | tf_op jit(solution)/shard_map/ppermute | solution.py:317
  47.0 3.4 %collective-permute-start.3 = (bf16[1,128,1024]{2,1,0:T(8,128)(2,1)S(1)}, bf16[1,128,1024]{2,1,0:T(8,128)(2,1)S(1)}, u32[]{:S(2)}, u32[]{:S(2)}) collective-permute-start(bf16[1,128,1024]{2,1,0:T(8,128)(2,1)S(1)} %slice.4), channel_id=1, source_target_pairs={{8,12},{9,13},{10,14},{11,15},{24,28},{25,29},{26,30},{27,31}} | collective-permute-start | bytes 786440 | tf_op jit(solution)/shard_map/ppermute | solution.py:318
  50.4 13.6 %query_rows.1 = (bf16[512,512]{1,0:T(8,128)(2,1)}, f32[512,16]{1,0:T(8,128)}) custom-call(s32[4]{0:T(128)} %len_ref.7, bf16[128,4,4096]{2,1,0:T(4,128)(2,1)} %x_ref.3, bf16[4096,512]{1,0:T(8,128)(2,1)} %wq_ref.1, bf16[16,4096]{1,0:T(8,128)(2,1)} %bitcast.21), custom_call_target="tpu_custom_call" | custom-call | tf_op jit(solution)/shard_map/query_rows/pallas_call | solution.py:321
  64.1 0.8 copy-done.3
  64.9 18.4 %attend.1 = bf16[4,128,512]{2,1,0:T(8,128)(2,1)} custom-call(s32[4]{0:T(128)} %len_ref.7, s32[1]{0:T(128)} %bitcast.4.pos_ref, bf16[4,128,512]{2,1,0:T(8,128)(2,1)} %bitcast.19, f32[4,128,16]{2,1,0:T(8,128)} %bitcast.20, bf16[2,128,1024]{2,1,0:T(8,128)(2,1)} %get-tuple-element.15.long_ref, bf16[2,128,1024]{2,1,0:T(8,128)(2,1)} %get-tuple-element.16.short_ref, ...), custom_call_target="tpu_custom_call" | custom-call | tf_op jit(solution)/shard_map/attend/pallas_call | solution.py:348
  83.3 1.2 collective-permute-start.4
  84.5 2.9 %collective-permute-start.6 = (bf16[512,512]{1,0:T(8,128)(2,1)}, bf16[512,512]{1,0:T(8,128)(2,1)S(1)}, u32[]{:S(2)}, u32[]{:S(2)}) collective-permute-start(bf16[512,512]{1,0:T(8,128)(2,1)} %bitcast.17), channel_id=1, source_target_pairs={{0,1},{1,0},{2,3},{3,2},{4,5},{5,4},{6,7},{7,6},{8,9},{9,8},{10,11... | collective-permute-start | bytes 1572872 | tf_op jit(solution)/shard_map/ppermute | solution.py:362
  87.5 6.9 %collective-permute-done.4.a_ref = bf16[512,512]{1,0:T(8,128)(2,1)S(1)} collective-permute-done((bf16[512,512]{1,0:T(8,128)(2,1)}, bf16[512,512]{1,0:T(8,128)(2,1)S(1)}, u32[]{:S(2)}, u32[]{:S(2)}) %collective-permute-start.4) | collective-permute-done | bytes 524320 | tf_op jit(solution)/shard_map/ppermute | solution.py:362
  94.3 3.5 %collective-permute-start.5 = (bf16[512,512]{1,0:T(8,128)(2,1)S(1)}, bf16[512,512]{1,0:T(8,128)(2,1)S(1)}, u32[]{:S(2)}, u32[]{:S(2)}) collective-permute-start(bf16[512,512]{1,0:T(8,128)(2,1)S(1)} %collective-permute-done.4.a_ref), channel_id=1, source_target_pairs={{0,1},{1,0},{2,3},{3,2},{4,5},{5,4},{6,7},{7,6},{8,9},{9,8},{10,11... | collective-permute-start | bytes 1572872 | tf_op jit(solution)/shard_map/ppermute | solution.py:362
  98.5 0.8 copy-done.5
  99.3 5.1 %near_heads.1.near_ref = f32[512,1024]{1,0:T(8,128)} custom-call(s32[4]{0:T(128)} %pad_add_fusion.idx_ref, bf16[512,512]{1,0:T(8,128)(2,1)} %bitcast.18, bf16[512,512]{1,0:T(8,128)(2,1)} %copy-done.5, bf16[4,512,1024]{2,1,0:T(8,128)(2,1)} %bitcast.12, bf16[4,512,1024]{2,1,0:T(8,128)(2,1)} %bitcast.13), custom_call_target="tpu_custom_call" | custom-call | tf_op jit(solution)/shard_map/near_heads/pallas_call | solution.py:373
  104.4 0.8 copy-done.4
  105.2 5.5 %far_heads.1 = (bf16[4,32,1024]{2,1,0:T(8,128)(2,1)}, bf16[4,32,1024]{2,1,0:T(8,128)(2,1)}, bf16[4,32,1024]{2,1,0:T(8,128)(2,1)}, bf16[4,32,1024]{2,1,0:T(8,128)(2,1)}) custom-call(s32[4]{0:T(128)} %pad_add_fusion.idx_ref, bf16[512,512]{1,0:T(8,128)(2,1)} %copy-done.2, bf16[512,512]{1,0:T(8,128)(2,1)} %copy-done.4, bf16[4,512,1024]{2,1,0:T(8,128)(2,1)} %bitcast.14, ...), custom_call_target="tpu_custom_call" | custom-call | tf_op jit(solution)/shard_map/far_heads/pallas_call | solution.py:386
  110.8 1.2 collective-permute-start.8
  112.0 0.9 collective-permute-start.9
  112.9 5.6 %collective-permute-done.8.refs_2_ = bf16[4,32,1024]{2,1,0:T(8,128)(2,1)S(1)} collective-permute-done((bf16[4,32,1024]{2,1,0:T(8,128)(2,1)}, bf16[4,32,1024]{2,1,0:T(8,128)(2,1)S(1)}, u32[]{:S(2)}, u32[]{:S(2)}) %collective-permute-start.8) | collective-permute-done | bytes 262176 | tf_op jit(solution)/shard_map/ppermute | solution.py:362
  118.5 6.2 %collective-permute-done.9.refs_3_ = bf16[4,32,1024]{2,1,0:T(8,128)(2,1)S(1)} collective-permute-done((bf16[4,32,1024]{2,1,0:T(8,128)(2,1)}, bf16[4,32,1024]{2,1,0:T(8,128)(2,1)S(1)}, u32[]{:S(2)}, u32[]{:S(2)}) %collective-permute-start.9) | collective-permute-done | bytes 262176 | tf_op jit(solution)/shard_map/ppermute | solution.py:362
  124.7 0.7 copy-done.9
  125.4 3.4 %place.1 = bf16[32,4,4096]{2,1,0:T(4,128)(2,1)} custom-call(s32[4]{0:T(128)} %len_ref.7, s32[4]{0:T(128)} %pad_add_fusion.idx_ref, bf16[4,32,1024]{2,1,0:T(8,128)(2,1)} %get-tuple-element.17.refs_0_, bf16[4,32,1024]{2,1,0:T(8,128)(2,1)} %copy-done.7, bf16[4,32,1024]{2,1,0:T(8,128)(2,1)} %copy-done.8, bf16[4,32,1024]{2,1,0:T(8,128)(2,1)} %copy-done.9), custom_call_target="tpu_custom_call" | custom-call | tf_op jit(solution)/shard_map/place/pallas_call | solution.py:401
  (24 shorter events, 0.8 us)
Async XLA Ops:
  18.2 14.9 %collective-permute-start = (bf16[2,128,1024]{2,1,0:T(8,128)(2,1)}, bf16[2,128,1024]{2,1,0:T(8,128)(2,1)S(1)}, u32[]{:S(2)}, u32[]{:S(2)}) collective-permute-start(bf16[2,128,1024]{2,1,0:T(8,128)(2,1)} %get-tuple-element.15.long_ref), channel_id=1, source_target_pairs={{0,4},{4,8},{8,12},{1,5},{5,9},{9,13},{2,6},{6,10},{10,14},{3,7},{... | collective-permute-start | bytes 1572872 | tf_op jit(solution)/shard_map/ppermute | solution.py:315
  33.1 30.9 %copy-start.1 = (bf16[2,128,1024]{2,1,0:T(8,128)(2,1)}, bf16[2,128,1024]{2,1,0:T(8,128)(2,1)S(1)}, u32[]{:S(2)}) copy-start(bf16[2,128,1024]{2,1,0:T(8,128)(2,1)S(1)} %collective-permute-done.a_ref) | copy-start | bytes 1572868
  33.1 13.8 %collective-permute-start.2 = (bf16[2,128,1024]{2,1,0:T(8,128)(2,1)S(1)}, bf16[2,128,1024]{2,1,0:T(8,128)(2,1)S(1)}, u32[]{:S(2)}, u32[]{:S(2)}) collective-permute-start(bf16[2,128,1024]{2,1,0:T(8,128)(2,1)S(1)} %collective-permute-done.a_ref), channel_id=1, source_target_pairs={{4,8},{8,12},{5,9},{9,13},{6,10},{10,14},{7,11},{11,15},{20,24},{2... | collective-permute-start | bytes 1572872 | tf_op jit(solution)/shard_map/ppermute | solution.py:317
  36.3 27.7 %collective-permute-start.1 = (bf16[2,128,1024]{2,1,0:T(8,128)(2,1)}, bf16[2,128,1024]{2,1,0:T(8,128)(2,1)S(1)}, u32[]{:S(2)}, u32[]{:S(2)}) collective-permute-start(bf16[2,128,1024]{2,1,0:T(8,128)(2,1)} %get-tuple-element.16.short_ref), channel_id=1, source_target_pairs={{0,4},{1,5},{2,6},{3,7},{16,20},{17,21},{18,22},{19,23}} | collective-permute-start | bytes 1572872 | tf_op jit(solution)/shard_map/ppermute | solution.py:316
  46.9 17.1 %copy-start = (bf16[2,128,1024]{2,1,0:T(8,128)(2,1)}, bf16[2,128,1024]{2,1,0:T(8,128)(2,1)S(1)}, u32[]{:S(2)}) copy-start(bf16[2,128,1024]{2,1,0:T(8,128)(2,1)S(1)} %collective-permute-done.2.c_ref) | copy-start | bytes 1572868
  47.0 17.1 %collective-permute-start.3 = (bf16[1,128,1024]{2,1,0:T(8,128)(2,1)S(1)}, bf16[1,128,1024]{2,1,0:T(8,128)(2,1)S(1)}, u32[]{:S(2)}, u32[]{:S(2)}) collective-permute-start(bf16[1,128,1024]{2,1,0:T(8,128)(2,1)S(1)} %slice.4), channel_id=1, source_target_pairs={{8,12},{9,13},{10,14},{11,15},{24,28},{25,29},{26,30},{27,31}} | collective-permute-start | bytes 786440 | tf_op jit(solution)/shard_map/ppermute | solution.py:318
  64.0 0.8 copy-start.3
  64.0 0.9 copy-start.6
  83.3 11.0 %collective-permute-start.4 = (bf16[512,512]{1,0:T(8,128)(2,1)}, bf16[512,512]{1,0:T(8,128)(2,1)S(1)}, u32[]{:S(2)}, u32[]{:S(2)}) collective-permute-start(bf16[512,512]{1,0:T(8,128)(2,1)} %bitcast.16), channel_id=1, source_target_pairs={{0,2},{1,3},{2,0},{3,1},{4,6},{5,7},{6,4},{7,5},{8,10},{9,11},{10,... | collective-permute-start | bytes 1572872 | tf_op jit(solution)/shard_map/ppermute | solution.py:362
  84.5 14.0 %collective-permute-start.6 = (bf16[512,512]{1,0:T(8,128)(2,1)}, bf16[512,512]{1,0:T(8,128)(2,1)S(1)}, u32[]{:S(2)}, u32[]{:S(2)}) collective-permute-start(bf16[512,512]{1,0:T(8,128)(2,1)} %bitcast.17), channel_id=1, source_target_pairs={{0,1},{1,0},{2,3},{3,2},{4,5},{5,4},{6,7},{7,6},{8,9},{9,8},{10,11... | collective-permute-start | bytes 1572872 | tf_op jit(solution)/shard_map/ppermute | solution.py:362
  94.3 10.1 %copy-start.2 = (bf16[512,512]{1,0:T(8,128)(2,1)}, bf16[512,512]{1,0:T(8,128)(2,1)S(1)}, u32[]{:S(2)}) copy-start(bf16[512,512]{1,0:T(8,128)(2,1)S(1)} %collective-permute-done.4.a_ref) | copy-start | bytes 1572868
  94.3 10.1 %collective-permute-start.5 = (bf16[512,512]{1,0:T(8,128)(2,1)S(1)}, bf16[512,512]{1,0:T(8,128)(2,1)S(1)}, u32[]{:S(2)}, u32[]{:S(2)}) collective-permute-start(bf16[512,512]{1,0:T(8,128)(2,1)S(1)} %collective-permute-done.4.a_ref), channel_id=1, source_target_pairs={{0,1},{1,0},{2,3},{3,2},{4,5},{5,4},{6,7},{7,6},{8,9},{9,8},{10,11... | collective-permute-start | bytes 1572872 | tf_op jit(solution)/shard_map/ppermute | solution.py:362
  98.5 0.8 copy-start.5
  104.4 0.8 copy-start.4
  110.8 2.1 %collective-permute-start.7 = (bf16[4,32,1024]{2,1,0:T(8,128)(2,1)}, bf16[4,32,1024]{2,1,0:T(8,128)(2,1)S(1)}, u32[]{:S(2)}, u32[]{:S(2)}) collective-permute-start(bf16[4,32,1024]{2,1,0:T(8,128)(2,1)} %get-tuple-element.18), channel_id=1, source_target_pairs={{0,1},{1,0},{2,3},{3,2},{4,5},{5,4},{6,7},{7,6},{8,9},{9,8},{10,11... | collective-permute-start | bytes 786440 | tf_op jit(solution)/shard_map/ppermute | solution.py:362
  110.8 7.6 %collective-permute-start.8 = (bf16[4,32,1024]{2,1,0:T(8,128)(2,1)}, bf16[4,32,1024]{2,1,0:T(8,128)(2,1)S(1)}, u32[]{:S(2)}, u32[]{:S(2)}) collective-permute-start(bf16[4,32,1024]{2,1,0:T(8,128)(2,1)} %get-tuple-element.19), channel_id=1, source_target_pairs={{0,2},{1,3},{2,0},{3,1},{4,6},{5,7},{6,4},{7,5},{8,10},{9,11},{10,... | collective-permute-start | bytes 786440 | tf_op jit(solution)/shard_map/ppermute | solution.py:362
  112.0 12.7 %collective-permute-start.9 = (bf16[4,32,1024]{2,1,0:T(8,128)(2,1)}, bf16[4,32,1024]{2,1,0:T(8,128)(2,1)S(1)}, u32[]{:S(2)}, u32[]{:S(2)}) collective-permute-start(bf16[4,32,1024]{2,1,0:T(8,128)(2,1)} %get-tuple-element.20), channel_id=1, source_target_pairs={{0,3},{1,2},{2,1},{3,0},{4,7},{5,6},{6,5},{7,4},{8,11},{9,10},{10,... | collective-permute-start | bytes 786440 | tf_op jit(solution)/shard_map/ppermute | solution.py:362
  112.9 11.8 %copy-start.7 = (bf16[4,32,1024]{2,1,0:T(8,128)(2,1)}, bf16[4,32,1024]{2,1,0:T(8,128)(2,1)S(1)}, u32[]{:S(2)}) copy-start(bf16[4,32,1024]{2,1,0:T(8,128)(2,1)S(1)} %collective-permute-done.7.refs_1_) | copy-start | bytes 786436
  118.5 6.2 %copy-start.8 = (bf16[4,32,1024]{2,1,0:T(8,128)(2,1)}, bf16[4,32,1024]{2,1,0:T(8,128)(2,1)S(1)}, u32[]{:S(2)}) copy-start(bf16[4,32,1024]{2,1,0:T(8,128)(2,1)S(1)} %collective-permute-done.8.refs_2_) | copy-start | bytes 786436
  124.7 0.7 copy-start.9

commit v2 on v1

--- a/solution.py
+++ b/solution.py
@@ -6,6 +6,7 @@
 from jax.experimental import pallas as pl
 from jax.experimental.pallas import tpu as pltpu
 from jax.sharding import PartitionSpec as P
+
 
 HD = 64
 QB = 64
@@ -105,7 +106,7 @@
     step_fn = partial(
         fold_step, queries=queries, chosen=chosen, query_pos=query_pos, lengths=lengths
     )
-    maxima, totals, weighted = step_fn(
+    _, totals, weighted = step_fn(
         start_state,
         (
             lax.all_gather(key_rows, "kv", axis=0, tiled=True),
@@ -151,12 +152,15 @@
     return lens, ranks
 
 
-def sort_rows(len_ref, x_ref, rows_ref):
-    row_count, seq_count, _ = x_ref.shape
+def sorted_sources(len_ref, seq_count):
     _, ranks = length_ranks(len_ref, seq_count)
-    for s in range(seq_count):
-        start = pl.multiple_of(ranks[s] * row_count, row_count)
-        rows_ref[pl.ds(start, row_count), :] = x_ref[:, s, :]
+    sources = []
+    for r in range(seq_count):
+        source = jnp.int32(0)
+        for s in range(1, seq_count):
+            source = source + jnp.where(ranks[s] == r, s, 0)
+        sources.append(source)
+    return sources
 
 
 def dot32(a, b):
@@ -167,41 +171,59 @@
     return lax.dot_general(a, b, (((1,), (1,)), ((), ())), preferred_element_type=jnp.float32)
 
 
-def kv_kernel(len_ref, x_ref, wk_ref, wv_ref, long_ref, short_ref, rows_ref):
-    step = pl.program_id(0)
-    half = pl.num_programs(0) // 2
-
-    @pl.when(step == 0)
+def flat_lanes(rows_ref):
+    return jnp.concatenate([rows_ref[i] for i in range(rows_ref.shape[0])], axis=1)
+
+
+def store_sorted(len_ref, acc_ref, product, out_refs):
+    seq_count = sum(o.shape[0] for o in out_refs)
+    row_count = out_refs[0].shape[1]
+    lanes = acc_ref.shape[-1]
+    for c in range(acc_ref.shape[0]):
+        acc_ref[c] = product[:, c * lanes : (c + 1) * lanes]
+    sources = sorted_sources(len_ref, seq_count)
+    r = 0
+    for out_ref in out_refs:
+        for at in range(out_ref.shape[0]):
+            out_ref[at] = jnp.concatenate(
+                [
+                    acc_ref[c, pl.ds(sources[r], row_count, stride=seq_count), :]
+                    for c in range(acc_ref.shape[0])
+                ],
+                axis=1,
+            ).astype(out_ref.dtype)
+            r += 1
+
+
+def first_kernel(len_ref, x_ref, w_ref, long_ref, short_ref, rows_ref, acc_ref):
+    tile_count, flat, lanes = rows_ref.shape
+
+    @pl.when(pl.program_id(0) == 0)
     def _():
-        sort_rows(len_ref, x_ref, rows_ref)
-
-    def emit(w_ref):
-        out = dot32(rows_ref[...], w_ref[...]).astype(jnp.bfloat16)
-        out = out.reshape((2,) + long_ref.shape[:2] + out.shape[1:])
-        long_ref[...] = out[0]
-        short_ref[...] = out[1]
-
-    @pl.when(step < half)
+        for i in range(tile_count):
+            rows_ref[i] = x_ref[:, :, i * lanes : (i + 1) * lanes].reshape(flat, lanes)
+
+    store_sorted(len_ref, acc_ref, dot32(flat_lanes(rows_ref), w_ref[...]), (long_ref, short_ref))
+
+
+def next_kernel(len_ref, rows_ref, w_ref, long_ref, short_ref, acc_ref):
+    store_sorted(len_ref, acc_ref, dot32(flat_lanes(rows_ref), w_ref[...]), (long_ref, short_ref))
+
+
+def q_kernel(len_ref, rows_ref, wq_ref, wg_ref, q_ref, gate_ref, acc_ref, gate_acc_ref):
+    rows = flat_lanes(rows_ref)
+
+    @pl.when(pl.program_id(0) == 0)
     def _():
-        emit(wk_ref)
-
-    @pl.when(step >= half)
-    def _():
-        emit(wv_ref)
-
-
-def q_kernel(len_ref, x_ref, wq_ref, wg_ref, q_ref, gate_ref, rows_ref):
-    step = pl.program_id(0)
-
-    @pl.when(step == 0)
-    def _():
-        sort_rows(len_ref, x_ref, rows_ref)
-        gate_ref[...] = jax.nn.sigmoid(dot_nt(rows_ref[...], wg_ref[...]))
-
-    q_ref[...] = dot32(rows_ref[...], wq_ref[...]).astype(jnp.bfloat16)
-
-
-def attend_kernel(len_ref, pos_ref, q_ref, gate_ref, long_ref, short_ref, a_ref, b_ref, c_ref, d_ref, pool_ref, out_ref):
+        store_sorted(len_ref, gate_acc_ref, jax.nn.sigmoid(dot_nt(rows, wg_ref[...])), (gate_ref,))
+
+    store_sorted(len_ref, acc_ref, dot32(rows, wq_ref[...]), (q_ref,))
+
+
+def attend_kernel(len_ref, pos_ref, q_ref, gate_ref, *refs):
+    own = (refs[0:2], refs[2:4])
+    got_a, got_b, got_c, got_d = refs[4:6], refs[6:8], refs[8:10], refs[10:12]
+    pool_ref, out_ref = refs[12:]
     seq_count, row_count, width = q_ref.shape
     head_count = width // HD
     lens, ranks = length_ranks(len_ref, seq_count)
@@ -210,56 +232,68 @@
     per_block = row_count // L_CMP
     row_id = lax.broadcasted_iota(jnp.int32, (row_count, 1), 0)
     tri = lax.broadcasted_iota(jnp.int32, (row_count, row_count), 1) <= row_id
-    cmp_end = lax.broadcasted_iota(jnp.int32, (row_count, per_block), 1) * L_CMP + L_CMP - 1
-    cmp_tri = cmp_end <= row_id
-    pool_rows = [
-        jnp.concatenate([pool_ref[i]] * head_count, axis=1) for i in range(2)
-    ]
-
-    def pooled(rows, weight):
+
+    def pooled(rows, which):
+        weight = jnp.concatenate([pool_ref[which]] * head_count, axis=1)
         grouped = rows.astype(jnp.float32).reshape(per_block, L_CMP, width)
         return (grouped * weight[None]).sum(1)
 
-    for r in range(seq_count):
-        length = jnp.int32(0)
-        for s in range(seq_count):
-            length = length + jnp.where(ranks[s] == r, lens[s], 0)
+    def one_sequence(r, length, pieces):
+        count = len(pieces)
+        join = lambda rows: rows[0] if count == 1 else jnp.concatenate(rows, axis=0)
+        key_rows = [k[at] for (k, v), at in pieces]
+        value_rows = [v[at] for (k, v), at in pieces]
+        keys, vals = join(key_rows), join(value_rows)
+        key_pool = join([pooled(p, 0) for p in key_rows]).astype(jnp.bfloat16)
+        val_pool = join([pooled(p, 1) for p in value_rows]).astype(jnp.bfloat16)
         live = block * row_count + row_id < length
-        if r == 0:
-            pieces = [long_ref[0], a_ref[0], c_ref[0], d_ref[0]]
-        elif r == 1:
-            pieces = [long_ref[1], a_ref[1], c_ref[1]]
-        else:
-            pieces = [short_ref[r - 2], b_ref[r - 2]]
-        keys = jnp.concatenate([p[:, :width] for p in pieces], axis=0)
-        vals = jnp.concatenate([p[:, width:] for p in pieces], axis=0)
-        key_pool = jnp.concatenate([pooled(p[:, :width], pool_rows[0]) for p in pieces], axis=0).astype(jnp.bfloat16)
-        val_pool = jnp.concatenate([pooled(p[:, width:], pool_rows[1]) for p in pieces], axis=0).astype(jnp.bfloat16)
-        usable = jnp.concatenate(
-            [tri] + [jnp.full((row_count, row_count), block >= i) for i in range(1, len(pieces))], axis=1
-        )
-        cmp_id = lax.broadcasted_iota(jnp.int32, (row_count, per_block * len(pieces)), 1)
-        cmp_blk = cmp_id // per_block
-        cmp_usable = ((cmp_blk == 0) & (cmp_id * L_CMP + L_CMP - 1 <= row_id)) | (
-            (cmp_blk > 0) & (cmp_blk <= block)
-        )
-
-        def soft(query, key, value, mask):
-            scores = jnp.where(mask, dot_nt(query, key) * scale, LOW_FILL)
-            top = jnp.max(scores, axis=1, keepdims=True)
-            weights = jnp.where(mask, jnp.exp(scores - top), 0.0)
-            total = jnp.sum(weights, axis=1, keepdims=True)
-            return dot32(weights.astype(jnp.bfloat16), value) / jnp.where(total > 0, total, 1.0)
-
+        cmp_id = lax.broadcasted_iota(jnp.int32, (row_count, per_block * count), 1)
+        cmp_usable = (cmp_id >= per_block) | (cmp_id * L_CMP + L_CMP - 1 <= row_id)
+        queries = q_ref[r]
+        gates = gate_ref[r]
         outs = []
         for h in range(head_count):
             cols = slice(h * HD, (h + 1) * HD)
-            query = q_ref[r][:, cols]
-            picked = soft(query, keys[:, cols], vals[:, cols], usable)
-            pool = soft(query, key_pool[:, cols], val_pool[:, cols], cmp_usable)
-            mixed = gate_ref[r][:, h : h + 1] * pool + gate_ref[r][:, head_count + h : head_count + h + 1] * picked
-            outs.append(jnp.where(live, mixed, 0.0))
-        out_ref[r] = jnp.concatenate(outs, axis=1).astype(jnp.bfloat16)
+            query = queries[:, cols]
+            scores = dot_nt(query, keys[:, cols]) * scale
+            near = jnp.where(tri, scores[:, :row_count], LOW_FILL)
+            scores = near if count == 1 else jnp.concatenate([near, scores[:, row_count:]], axis=1)
+            weights = jnp.exp(scores - jnp.max(scores, axis=1, keepdims=True))
+            total = jnp.sum(weights, axis=1, keepdims=True)
+            picked = dot32(weights.astype(jnp.bfloat16), vals[:, cols])
+            scores = jnp.where(cmp_usable, dot_nt(query, key_pool[:, cols]) * scale, LOW_FILL)
+            weights = jnp.where(cmp_usable, jnp.exp(scores - jnp.max(scores, axis=1, keepdims=True)), 0.0)
+            cmp_total = jnp.sum(weights, axis=1, keepdims=True)
+            pool = dot32(weights.astype(jnp.bfloat16), val_pool[:, cols])
+            pool_gate = gates[:, h : h + 1] / jnp.where(cmp_total > 0, cmp_total, 1.0)
+            pick_gate = gates[:, head_count + h : head_count + h + 1] / total
+            outs.append(pool_gate * pool + pick_gate * picked)
+        mixed = jnp.where(live, jnp.concatenate(outs, axis=1), 0.0)
+        out_ref[r] = mixed.astype(jnp.bfloat16)
+
+    def pair_of(base, sources):
+        def one(at, carry):
+            r = base + at
+            length = jnp.int32(0)
+            for s in range(seq_count):
+                length = length + jnp.where(ranks[s] == r, lens[s], 0)
+            alive = block * row_count < length
+
+            @pl.when(jnp.logical_not(alive))
+            def _():
+                out_ref[r] = jnp.zeros((row_count, width), jnp.bfloat16)
+
+            for count in range(1, len(sources) + 1):
+                @pl.when(alive & (block == count - 1))
+                def _():
+                    one_sequence(r, length, [(x, at if x[0].shape[0] > 1 else 0) for x in sources[:count]])
+
+            return carry
+
+        lax.fori_loop(0, own[0][0].shape[0], one, 0)
+
+    pair_of(0, [own[0], got_a, got_c, got_d])
+    pair_of(own[0][0].shape[0], [own[1], got_b])
 
 
 def part_product(rows_ref, w_ref):
@@ -272,7 +306,6 @@
 
 def far_kernel(idx_ref, a_ref, b_ref, wa_ref, wb_ref, near_ref, *out_refs):
     total = near_ref[...] + (part_product(a_ref, wa_ref) + part_product(b_ref, wb_ref))
-    seq_count, row_count, width = out_refs[-1].shape
     out_refs[-1][...] = total.astype(jnp.bfloat16).reshape(out_refs[-1].shape)
     piece = out_refs[0].shape[1]
     for k in range(len(out_refs) - 1):
@@ -280,7 +313,7 @@
         out_refs[k][...] = out_refs[-1][:, pl.ds(start, piece), :]
 
 
-def live_body(tokens, lengths, chosen, w_query, w_key, w_value, w_gate, pool_weights, w_out):
+def live_body(tokens, lengths, w_query, w_key, w_value, w_gate, pool_weights, w_out):
     row_count, seq_count, model_width = tokens.shape
     width = w_query.shape[1]
     head_count = width // HD
@@ -294,57 +327,82 @@
     params = pltpu.CompilerParams(vmem_limit_bytes=56 * 2**20, dimension_semantics=("arbitrary",))
     whole = lambda shape: pl.BlockSpec(shape, lambda *_: (0,) * len(shape))
 
-    kv_long, kv_short = pl.pallas_call(
-        kv_kernel,
+    lanes = 128
+    tiles = model_width // lanes
+    rows_shape = jax.ShapeDtypeStruct((tiles, flat, lanes), bf16)
+    pair_shape = [jax.ShapeDtypeStruct((two, row_count, width), bf16)] * 2
+    pair_spec = [pl.BlockSpec((two, row_count, half), lambda i, n: (0, 0, i))] * 2
+    half_spec = pl.BlockSpec((model_width, half), lambda i, n: (0, i))
+    acc = pltpu.VMEM((half // lanes, flat, lanes), jnp.float32)
+    cost = lambda out_cols, k: pl.CostEstimate(flops=2 * flat * out_cols * k, bytes_accessed=2 * out_cols * k, transcendentals=0)
+
+    key_long, key_short, rows = pl.pallas_call(
+        first_kernel,
         grid_spec=pltpu.PrefetchScalarGridSpec(
             num_scalar_prefetch=1,
-            grid=(4,),
-            in_specs=[
-                pl.BlockSpec(tokens.shape, lambda i, n: (0, 0, 0), pipeline_mode=pl.Buffered(1)),
-                pl.BlockSpec((model_width, half), lambda i, n: (0, jnp.minimum(i, 1))),
-                pl.BlockSpec((model_width, half), lambda i, n: (0, jnp.maximum(i - 2, 0))),
-            ],
-            out_specs=[pl.BlockSpec((two, row_count, half), lambda i, n: (0, 0, i))] * 2,
-            scratch_shapes=[pltpu.VMEM((flat, model_width), bf16)],
-        ),
-        out_shape=[jax.ShapeDtypeStruct((two, row_count, 2 * width), bf16)] * 2,
+            grid=(2,),
+            in_specs=[pl.BlockSpec(tokens.shape, lambda i, n: (0, 0, 0), pipeline_mode=pl.Buffered(1)), half_spec],
+            out_specs=pair_spec + [whole(rows_shape.shape)],
+            scratch_shapes=[acc],
+        ),
+        out_shape=pair_shape + [rows_shape],
         compiler_params=params,
-        name="kv_rows",
-    )(lengths, tokens, w_key, w_value)
-
-    got_a = lax.ppermute(kv_long, "kv", [(0, 1), (1, 2), (2, 3)])
-    got_b = lax.ppermute(kv_short, "kv", [(0, 1)])
-    got_c = lax.ppermute(got_a, "kv", [(1, 2), (2, 3)])
-    got_d = lax.ppermute(got_c[:1], "kv", [(2, 3)])
+        cost_estimate=cost(width, model_width),
+        name="key_rows",
+    )(lengths, tokens, w_key)
+
+    def next_rows(weight):
+        return pl.pallas_call(
+            next_kernel,
+            grid_spec=pltpu.PrefetchScalarGridSpec(
+                num_scalar_prefetch=1,
+                grid=(2,),
+                in_specs=[whole(rows_shape.shape), half_spec],
+                out_specs=pair_spec,
+                scratch_shapes=[acc],
+            ),
+            out_shape=pair_shape,
+            compiler_params=params,
+            cost_estimate=cost(width, model_width),
+            name="value_rows",
+        )(lengths, rows, weight)
+
+    val_long, val_short = next_rows(w_value)
+
+    up = lambda x, pairs: lax.ppermute(x, "kv", pairs)
+    key_a = up(key_long, [(0, 1), (1, 2), (2, 3)])
+    val_a = up(val_long, [(0, 1), (1, 2), (2, 3)])
+    key_b = up(key_short, [(0, 1)])
+    key_c = up(key_a, [(1, 2), (2, 3)])
+    val_b = up(val_short, [(0, 1)])
+    val_c = up(val_a, [(1, 2), (2, 3)])
+    key_d = up(key_c[:1], [(2, 3)])
+    val_d = up(val_c[:1], [(2, 3)])
 
     gate_rows = w_gate.transpose(1, 2, 0).reshape(2 * head_count, model_width)
+    gate_rows = jnp.pad(gate_rows, ((0, lanes - 2 * head_count), (0, 0)))
     queries, gates = pl.pallas_call(
         q_kernel,
         grid_spec=pltpu.PrefetchScalarGridSpec(
             num_scalar_prefetch=1,
             grid=(2,),
-            in_specs=[
-                pl.BlockSpec(tokens.shape, lambda i, n: (0, 0, 0), pipeline_mode=pl.Buffered(1)),
-                pl.BlockSpec((model_width, half), lambda i, n: (0, i)),
-                whole(gate_rows.shape),
+            in_specs=[whole(rows_shape.shape), half_spec, whole(gate_rows.shape)],
+            out_specs=[
+                pl.BlockSpec((seq_count, row_count, half), lambda i, n: (0, 0, i)),
+                whole((seq_count, row_count, lanes)),
             ],
-            out_specs=[
-                pl.BlockSpec((flat, half), lambda i, n: (0, i)),
-                whole((flat, 2 * head_count)),
-            ],
-            scratch_shapes=[pltpu.VMEM((flat, model_width), bf16)],
+            scratch_shapes=[acc, pltpu.VMEM((1, flat, lanes), jnp.float32)],
         ),
         out_shape=[
-            jax.ShapeDtypeStruct((flat, width), bf16),
-            jax.ShapeDtypeStruct((flat, 2 * head_count), jnp.float32),
+            jax.ShapeDtypeStruct((seq_count, row_count, width), bf16),
+            jax.ShapeDtypeStruct((seq_count, row_count, lanes), jnp.float32),
         ],
         compiler_params=params,
+        cost_estimate=cost(width + lanes, model_width),
         name="query_rows",
-    )(lengths, tokens, w_query, gate_rows)
-    queries = queries.reshape(seq_count, row_count, width)
-    gates = gates.reshape(seq_count, row_count, 2 * head_count)
-
-    operands = (queries, gates, kv_long, kv_short, got_a, got_b, got_c, got_d, pool_weights)
+    )(lengths, rows, w_query, gate_rows)
+
+    operands = (queries, gates, key_long, val_long, key_short, val_short, key_a, val_a, key_b, val_b, key_c, val_c, key_d, val_d, pool_weights)
     attended = pl.pallas_call(
         attend_kernel,
         grid_spec=pltpu.PrefetchScalarGridSpec(
@@ -355,6 +413,7 @@
         ),
         out_shape=jax.ShapeDtypeStruct(queries.shape, bf16),
         compiler_params=params,
+        cost_estimate=cost(width, 2 * model_width),
         name="attend",
     )(lengths, kv_at[None], *operands)
 
@@ -380,6 +439,7 @@
         ),
         out_shape=jax.ShapeDtypeStruct((flat, col_width), jnp.float32),
         compiler_params=params,
+        cost_estimate=cost(col_width, 2 * width),
         name="near_heads",
     )(order, attended, near_b, weight, weight)
     piece = row_count // tp_size
@@ -394,6 +454,7 @@
         ),
         out_shape=[jax.ShapeDtypeStruct((seq_count, piece, col_width), bf16)] * tp_size,
         compiler_params=params,
+        cost_estimate=cost(col_width, 2 * width),
         name="far_heads",
     )(order, far_a, far_b, weight, weight, near)
     got = [parts[0]] + [swap(parts[k], k) for k in (2, 3, 1)]
@@ -414,7 +475,7 @@
 
 def place_kernel(len_ref, idx_ref, *refs):
     out_ref = refs[-1]
-    seq_count, piece, col_width = refs[0].shape
+    seq_count, _, col_width = refs[0].shape
     _, ranks = length_ranks(len_ref, seq_count)
     for k, part in enumerate(refs[:-1]):
         start = pl.multiple_of(idx_ref[k] * col_width, col_width)
@@ -430,7 +491,7 @@
     most = [live_total // (row_count * j + 1) for j in range(1, kv_size)]
     dense = seq_len // QB <= chosen.shape[-1]
     if dense and kv_size == 4 and seq_count == 4 and lax.axis_size("tp") == 4 and most[1] <= 2 and most[2] <= 1:
-        return live_body(tokens, lengths, chosen, *weights)
+        return live_body(tokens, lengths, *weights)
     return general_body(tokens, lengths, chosen, *weights)
 
 

time: 129 us -> 113 us (0.88)
  the two profiles are of different devices: /device:TPU:21 before, /device:TPU:1 now
where the time goes in v2:
time: 113 us
  Pallas kernels  54.4 us (48%)
  starting transfers between devices  29 us (26%)
  waiting for transfers between devices  24.5 us (22%)
  local copies, waits for them, and re-layouts  4.25 us (4%)
    ppermute x8, starting transfers between devices, live_body(): up = lambda x, pairs: lax.ppermute(x, 'kv', pairs)  18 us
    ppermute x6, waiting for transfers between devices, live_body(): lax.ppermute(x, 'tp', [(t, t ^ bit) for t in range(tp_size)])  17.6 us
    pallas_call x1, Pallas kernels, live_body(): pl.pallas_call(attend_kernel, grid_spec=pltpu.PrefetchScalarGridSpec(num_...  15.5 us
    ppermute x6, starting transfers between devices, live_body(): lax.ppermute(x, 'tp', [(t, t ^ bit) for t in range(tp_size)])  11 us
    pallas_call x1, Pallas kernels, live_body(): pl.pallas_call(q_kernel, grid_spec=pltpu.PrefetchScalarGridSpec(num_scala...  8.98 us
    pallas_call x1, Pallas kernels, live_body(): pl.pallas_call(first_kernel, grid_spec=pltpu.PrefetchScalarGridSpec(num_s...  8.84 us
    pallas_call x1, Pallas kernels, next_rows(): pl.pallas_call(next_kernel, grid_spec=pltpu.PrefetchScalarGridSpec(num_sc...  6.98 us
    ppermute x8, waiting for transfers between devices, live_body(): up = lambda x, pairs: lax.ppermute(x, 'kv', pairs)  6.9 us
  transfers between devices with their start and end apart: 14, of which 5 were waited for; matrix products, arithmetic and copies ran while one was open for 1% of the time, Pallas kernels for 13%

profile of v2, /device:TPU:1, one launch (start us, length us, event | category | flops | bytes accessed | tf_op | source)
XLA Modules:
  0.0 112.9 jit_solution(5387486316865529894)
XLA Ops:
  0.0 8.8 %key_rows.1 = (bf16[2,128,512]{2,1,0:T(8,128)(2,1)}, bf16[2,128,512]{2,1,0:T(8,128)(2,1)}, bf16[32,512,128]{2,1,0:T(8,128)(2,1)}) custom-call(s32[4]{0:T(128)} %len_ref.9, bf16[128,4,4096]{2,1,0:T(4,128)(2,1)} %x_ref.1, bf16[4096,512]{1,0:T(8,128)(2,1)} %w_ref.2), custom_call_target="tpu_custom_call" | custom-call | flops 2147483648 | bytes 4194304 | tf_op jit(solution)/shard_map/key_rows/pallas_call | solution.py:339
  8.9 7.0 %value_rows.1 = (bf16[2,128,512]{2,1,0:T(8,128)(2,1)}, bf16[2,128,512]{2,1,0:T(8,128)(2,1)}) custom-call(s32[4]{0:T(128)} %len_ref.9, bf16[32,512,128]{2,1,0:T(8,128)(2,1)} %get-tuple-element.16.rows_ref, bf16[4096,512]{1,0:T(8,128)(2,1)} %w_ref.3), custom_call_target="tpu_custom_call" | custom-call | flops 2147483648 | bytes 4194304 | tf_op jit(solution)/shard_map/value_rows/pallas_call | solution.py:355
  15.8 4.0 %collective-permute-start.1 = (bf16[2,128,512]{2,1,0:T(8,128)(2,1)}, bf16[2,128,512]{2,1,0:T(8,128)(2,1)S(1)}, u32[]{:S(2)}, u32[]{:S(2)}) collective-permute-start(bf16[2,128,512]{2,1,0:T(8,128)(2,1)} %get-tuple-element.20.refs_1_), channel_id=1, source_target_pairs={{0,4},{4,8},{8,12},{1,5},{5,9},{9,13},{2,6},{6,10},{10,14},{3,7},{... | collective-permute-start | bytes 786440 | tf_op jit(solution)/shard_map/ppermute | solution.py:372
  19.9 3.2 %collective-permute-start = (bf16[2,128,512]{2,1,0:T(8,128)(2,1)S(1)}, bf16[2,128,512]{2,1,0:T(8,128)(2,1)S(1)}, u32[]{:S(2)}, u32[]{:S(2)}) collective-permute-start(bf16[2,128,512]{2,1,0:T(8,128)(2,1)S(1)} %copy-done.9), channel_id=1, source_target_pairs={{0,4},{4,8},{8,12},{1,5},{5,9},{9,13},{2,6},{6,10},{10,14},{3,7},{... | collective-permute-start | bytes 786440 | tf_op jit(solution)/shard_map/ppermute | solution.py:372
  23.1 2.0 %collective-permute-done.1.refs_5_ = bf16[2,128,512]{2,1,0:T(8,128)(2,1)S(1)} collective-permute-done((bf16[2,128,512]{2,1,0:T(8,128)(2,1)}, bf16[2,128,512]{2,1,0:T(8,128)(2,1)S(1)}, u32[]{:S(2)}, u32[]{:S(2)}) %collective-permute-start.1) | collective-permute-done | bytes 262176 | tf_op jit(solution)/shard_map/ppermute | solution.py:372
  25.8 4.8 %collective-permute-done.refs_4_ = bf16[2,128,512]{2,1,0:T(8,128)(2,1)S(1)} collective-permute-done((bf16[2,128,512]{2,1,0:T(8,128)(2,1)S(1)}, bf16[2,128,512]{2,1,0:T(8,128)(2,1)S(1)}, u32[]{:S(2)}, u32[]{:S(2)}) %collective-permute-start) | collective-permute-done | bytes 262176 | tf_op jit(solution)/shard_map/ppermute | solution.py:372
  31.3 6.7 %collective-permute-start.3 = (bf16[2,128,512]{2,1,0:T(8,128)(2,1)}, bf16[2,128,512]{2,1,0:T(8,128)(2,1)S(1)}, u32[]{:S(2)}, u32[]{:S(2)}) collective-permute-start(bf16[2,128,512]{2,1,0:T(8,128)(2,1)} %get-tuple-element.22.refs_3_), channel_id=1, source_target_pairs={{0,4},{1,5},{2,6},{3,7},{16,20},{17,21},{18,22},{19,23}} | collective-permute-start | bytes 786440 | tf_op jit(solution)/shard_map/ppermute | solution.py:372
  38.0 1.3 %collective-permute-start.2 = (bf16[2,128,512]{2,1,0:T(8,128)(2,1)S(1)}, bf16[2,128,512]{2,1,0:T(8,128)(2,1)S(1)}, u32[]{:S(2)}, u32[]{:S(2)}) collective-permute-start(bf16[2,128,512]{2,1,0:T(8,128)(2,1)S(1)} %copy-done.10), channel_id=1, source_target_pairs={{0,4},{1,5},{2,6},{3,7},{16,20},{17,21},{18,22},{19,23}} | collective-permute-start | bytes 786440 | tf_op jit(solution)/shard_map/ppermute | solution.py:372
  39.3 1.1 pad.4.wg_ref
  41.1 0.8 collective-permute-start.6
  42.0 9.0 %query_rows.1 = (bf16[4,128,512]{2,1,0:T(8,128)(2,1)}, f32[4,128,128]{2,1,0:T(8,128)}) custom-call(s32[4]{0:T(128)} %len_ref.9, bf16[32,512,128]{2,1,0:T(8,128)(2,1)} %get-tuple-element.16.rows_ref, bf16[4096,512]{1,0:T(8,128)(2,1)} %wq_ref.1, bf16[128,4096]{1,0:T(8,128)(2,1)} %pad.4.wg_ref), custom_call_target="tpu_custom_call" | custom-call | flops 2684354560 | bytes 5242880 | tf_op jit(solution)/shard_map/query_rows/pallas_call | solution.py:384
  51.9 15.5 %attend.1 = bf16[4,128,512]{2,1,0:T(8,128)(2,1)} custom-call(s32[4]{0:T(128)} %len_ref.9, s32[1]{0:T(128)} %bitcast.4.pos_ref, bf16[4,128,512]{2,1,0:T(8,128)(2,1)} %get-tuple-element.17.q_ref, f32[4,128,128]{2,1,0:T(8,128)} %get-tuple-element.18.gate_ref, bf16[2,128,512]{2,1,0:T(8,128)(2,1)} %get-tuple-element.19.refs_0_, ...), custom_call_target="tpu_custom_call" | custom-call | flops 4294967296 | bytes 8388608 | tf_op jit(solution)/shard_map/attend/pallas_call | solution.py:406
  67.4 1.2 %collective-permute-start.8 = (bf16[512,512]{1,0:T(8,128)(2,1)}, bf16[512,512]{1,0:T(8,128)(2,1)S(1)}, u32[]{:S(2)}, u32[]{:S(2)}) collective-permute-start(bf16[512,512]{1,0:T(8,128)(2,1)} %bitcast.14), channel_id=1, source_target_pairs={{0,2},{1,3},{2,0},{3,1},{4,6},{5,7},{6,4},{7,5},{8,10},{9,11},{10,... | collective-permute-start | bytes 1572872 | tf_op jit(solution)/shard_map/ppermute | solution.py:421
  68.6 3.5 %collective-permute-start.10 = (bf16[512,512]{1,0:T(8,128)(2,1)}, bf16[512,512]{1,0:T(8,128)(2,1)S(1)}, u32[]{:S(2)}, u32[]{:S(2)}) collective-permute-start(bf16[512,512]{1,0:T(8,128)(2,1)} %bitcast.15), channel_id=1, source_target_pairs={{0,1},{1,0},{2,3},{3,2},{4,5},{5,4},{6,7},{7,6},{8,9},{9,8},{10,11... | collective-permute-start | bytes 1572872 | tf_op jit(solution)/shard_map/ppermute | solution.py:421
  72.1 5.7 %collective-permute-done.8.a_ref = bf16[512,512]{1,0:T(8,128)(2,1)S(1)} collective-permute-done((bf16[512,512]{1,0:T(8,128)(2,1)}, bf16[512,512]{1,0:T(8,128)(2,1)S(1)}, u32[]{:S(2)}, u32[]{:S(2)}) %collective-permute-start.8) | collective-permute-done | bytes 524320 | tf_op jit(solution)/shard_map/ppermute | solution.py:421
  77.8 4.1 %collective-permute-start.9 = (bf16[512,512]{1,0:T(8,128)(2,1)S(1)}, bf16[512,512]{1,0:T(8,128)(2,1)S(1)}, u32[]{:S(2)}, u32[]{:S(2)}) collective-permute-start(bf16[512,512]{1,0:T(8,128)(2,1)S(1)} %collective-permute-done.8.a_ref), channel_id=1, source_target_pairs={{0,1},{1,0},{2,3},{3,2},{4,5},{5,4},{6,7},{7,6},{8,9},{9,8},{10,11... | collective-permute-start | bytes 1572872 | tf_op jit(solution)/shard_map/ppermute | solution.py:421
  82.5 0.8 copy-done.2
  83.3 5.1 %near_heads.1.near_ref = f32[512,1024]{1,0:T(8,128)} custom-call(s32[4]{0:T(128)} %pad_add_fusion.idx_ref, bf16[512,512]{1,0:T(8,128)(2,1)} %bitcast.16, bf16[512,512]{1,0:T(8,128)(2,1)} %copy-done.2, bf16[4,512,1024]{2,1,0:T(8,128)(2,1)} %bitcast.10, bf16[4,512,1024]{2,1,0:T(8,128)(2,1)} %bitcast.11), custom_call_target="tpu_custom_call" | custom-call | flops 1073741824 | bytes 2097152 | tf_op jit(solution)/shard_map/near_heads/pallas_call | solution.py:432
  89.3 5.5 %far_heads.1 = (bf16[4,32,1024]{2,1,0:T(8,128)(2,1)}, bf16[4,32,1024]{2,1,0:T(8,128)(2,1)}, bf16[4,32,1024]{2,1,0:T(8,128)(2,1)}, bf16[4,32,1024]{2,1,0:T(8,128)(2,1)}) custom-call(s32[4]{0:T(128)} %pad_add_fusion.idx_ref, bf16[512,512]{1,0:T(8,128)(2,1)} %copy-done, bf16[512,512]{1,0:T(8,128)(2,1)} %copy-done.1, bf16[4,512,1024]{2,1,0:T(8,128)(2,1)} %bitcast.12, ...), custom_call_target="tpu_custom_call" | custom-call | flops 1073741824 | bytes 2097152 | tf_op jit(solution)/shard_map/far_heads/pallas_call | solution.py:446
  94.9 1.2 %collective-permute-start.12 = (bf16[4,32,1024]{2,1,0:T(8,128)(2,1)}, bf16[4,32,1024]{2,1,0:T(8,128)(2,1)S(1)}, u32[]{:S(2)}, u32[]{:S(2)}) collective-permute-start(bf16[4,32,1024]{2,1,0:T(8,128)(2,1)} %get-tuple-element.25), channel_id=1, source_target_pairs={{0,2},{1,3},{2,0},{3,1},{4,6},{5,7},{6,4},{7,5},{8,10},{9,11},{10,... | collective-permute-start | bytes 786440 | tf_op jit(solution)/shard_map/ppermute | solution.py:421
  96.1 0.8 collective-permute-start.13
  96.9 5.6 %collective-permute-done.12.refs_2_ = bf16[4,32,1024]{2,1,0:T(8,128)(2,1)S(1)} collective-permute-done((bf16[4,32,1024]{2,1,0:T(8,128)(2,1)}, bf16[4,32,1024]{2,1,0:T(8,128)(2,1)S(1)}, u32[]{:S(2)}, u32[]{:S(2)}) %collective-permute-start.12) | collective-permute-done | bytes 262176 | tf_op jit(solution)/shard_map/ppermute | solution.py:421
  102.6 6.2 %collective-permute-done.13.refs_3_ = bf16[4,32,1024]{2,1,0:T(8,128)(2,1)S(1)} collective-permute-done((bf16[4,32,1024]{2,1,0:T(8,128)(2,1)}, bf16[4,32,1024]{2,1,0:T(8,128)(2,1)S(1)}, u32[]{:S(2)}, u32[]{:S(2)}) %collective-permute-start.13) | collective-permute-done | bytes 262176 | tf_op jit(solution)/shard_map/ppermute | solution.py:421
  109.5 3.4 %place.1 = bf16[32,4,4096]{2,1,0:T(4,128)(2,1)} custom-call(s32[4]{0:T(128)} %len_ref.9, s32[4]{0:T(128)} %pad_add_fusion.idx_ref, bf16[4,32,1024]{2,1,0:T(8,128)(2,1)} %get-tuple-element.23.refs_0_, bf16[4,32,1024]{2,1,0:T(8,128)(2,1)} %copy-done.3, bf16[4,32,1024]{2,1,0:T(8,128)(2,1)} %copy-done.4, bf16[4,32,1024]{2,1,0:T(8,128)(2,1)} %copy-done.5), custom_call_target="tpu_custom_call" | custom-call | tf_op jit(solution)/shard_map/place/pallas_call | solution.py:462
  (49 shorter events, 5.1 us)
Async XLA Ops:
  8.8 11.0 %copy-start.9 = (bf16[2,128,512]{2,1,0:T(8,128)(2,1)S(1)}, bf16[2,128,512]{2,1,0:T(8,128)(2,1)}, u32[]{:S(2)}) copy-start(bf16[2,128,512]{2,1,0:T(8,128)(2,1)} %get-tuple-element.19.refs_0_) | copy-start | bytes 786436
  8.8 29.1 %copy-start.10 = (bf16[2,128,512]{2,1,0:T(8,128)(2,1)S(1)}, bf16[2,128,512]{2,1,0:T(8,128)(2,1)}, u32[]{:S(2)}) copy-start(bf16[2,128,512]{2,1,0:T(8,128)(2,1)} %get-tuple-element.21.refs_2_) | copy-start | bytes 786436
  8.8 30.5 %copy-start.6 = (bf16[4096,2,8]{0,2,1:T(8,128)(2,1)S(1)}, bf16[4096,2,8]{0,2,1:T(8,128)(2,1)}, u32[]{:S(2)}) copy-start(bf16[4096,2,8]{0,2,1:T(8,128)(2,1)} %param.14) | copy-start | bytes 393220
  15.8 9.3 %collective-permute-start.1 = (bf16[2,128,512]{2,1,0:T(8,128)(2,1)}, bf16[2,128,512]{2,1,0:T(8,128)(2,1)S(1)}, u32[]{:S(2)}, u32[]{:S(2)}) collective-permute-start(bf16[2,128,512]{2,1,0:T(8,128)(2,1)} %get-tuple-element.20.refs_1_), channel_id=1, source_target_pairs={{0,4},{4,8},{8,12},{1,5},{5,9},{9,13},{2,6},{6,10},{10,14},{3,7},{... | collective-permute-start | bytes 786440 | tf_op jit(solution)/shard_map/ppermute | solution.py:372
  19.9 10.8 %collective-permute-start = (bf16[2,128,512]{2,1,0:T(8,128)(2,1)S(1)}, bf16[2,128,512]{2,1,0:T(8,128)(2,1)S(1)}, u32[]{:S(2)}, u32[]{:S(2)}) collective-permute-start(bf16[2,128,512]{2,1,0:T(8,128)(2,1)S(1)} %copy-done.9), channel_id=1, source_target_pairs={{0,4},{4,8},{8,12},{1,5},{5,9},{9,13},{2,6},{6,10},{10,14},{3,7},{... | collective-permute-start | bytes 786440 | tf_op jit(solution)/shard_map/ppermute | solution.py:372
  25.1 25.8 %copy-start.11 = (bf16[2,128,512]{2,1,0:T(8,128)(2,1)}, bf16[2,128,512]{2,1,0:T(8,128)(2,1)S(1)}, u32[]{:S(2)}) copy-start(bf16[2,128,512]{2,1,0:T(8,128)(2,1)S(1)} %collective-permute-done.1.refs_5_) | copy-start | bytes 786436
  25.1 15.3 %collective-permute-start.5 = (bf16[2,128,512]{2,1,0:T(8,128)(2,1)S(1)}, bf16[2,128,512]{2,1,0:T(8,128)(2,1)S(1)}, u32[]{:S(2)}, u32[]{:S(2)}) collective-permute-start(bf16[2,128,512]{2,1,0:T(8,128)(2,1)S(1)} %collective-permute-done.1.refs_5_), channel_id=1, source_target_pairs={{4,8},{8,12},{5,9},{9,13},{6,10},{10,14},{7,11},{11,15},{20,24},{2... | collective-permute-start | bytes 786440 | tf_op jit(solution)/shard_map/ppermute | solution.py:372
  30.6 20.3 %copy-start.12 = (bf16[2,128,512]{2,1,0:T(8,128)(2,1)}, bf16[2,128,512]{2,1,0:T(8,128)(2,1)S(1)}, u32[]{:S(2)}) copy-start(bf16[2,128,512]{2,1,0:T(8,128)(2,1)S(1)} %collective-permute-done.refs_4_) | copy-start | bytes 786436
  30.6 10.4 %collective-permute-start.4 = (bf16[2,128,512]{2,1,0:T(8,128)(2,1)S(1)}, bf16[2,128,512]{2,1,0:T(8,128)(2,1)S(1)}, u32[]{:S(2)}, u32[]{:S(2)}) collective-permute-start(bf16[2,128,512]{2,1,0:T(8,128)(2,1)S(1)} %collective-permute-done.refs_4_), channel_id=1, source_target_pairs={{4,8},{8,12},{5,9},{9,13},{6,10},{10,14},{7,11},{11,15},{20,24},{2... | collective-permute-start | bytes 786440 | tf_op jit(solution)/shard_map/ppermute | solution.py:372
  31.3 19.7 %collective-permute-start.3 = (bf16[2,128,512]{2,1,0:T(8,128)(2,1)}, bf16[2,128,512]{2,1,0:T(8,128)(2,1)S(1)}, u32[]{:S(2)}, u32[]{:S(2)}) collective-permute-start(bf16[2,128,512]{2,1,0:T(8,128)(2,1)} %get-tuple-element.22.refs_3_), channel_id=1, source_target_pairs={{0,4},{1,5},{2,6},{3,7},{16,20},{17,21},{18,22},{19,23}} | collective-permute-start | bytes 786440 | tf_op jit(solution)/shard_map/ppermute | solution.py:372
  38.0 13.0 %collective-permute-start.2 = (bf16[2,128,512]{2,1,0:T(8,128)(2,1)S(1)}, bf16[2,128,512]{2,1,0:T(8,128)(2,1)S(1)}, u32[]{:S(2)}, u32[]{:S(2)}) collective-permute-start(bf16[2,128,512]{2,1,0:T(8,128)(2,1)S(1)} %copy-done.10), channel_id=1, source_target_pairs={{0,4},{1,5},{2,6},{3,7},{16,20},{17,21},{18,22},{19,23}} | collective-permute-start | bytes 786440 | tf_op jit(solution)/shard_map/ppermute | solution.py:372
  40.4 10.6 %copy-start.7 = (bf16[2,128,512]{2,1,0:T(8,128)(2,1)}, bf16[2,128,512]{2,1,0:T(8,128)(2,1)S(1)}, u32[]{:S(2)}) copy-start(bf16[2,128,512]{2,1,0:T(8,128)(2,1)S(1)} %collective-permute-done.5.refs_9_) | copy-start | bytes 786436
  40.4 10.6 %collective-permute-start.7 = (bf16[1,128,512]{2,1,0:T(8,128)(2,1)S(1)}, bf16[1,128,512]{2,1,0:T(8,128)(2,1)S(1)}, u32[]{:S(2)}, u32[]{:S(2)}) collective-permute-start(bf16[1,128,512]{2,1,0:T(8,128)(2,1)S(1)} %slice.9), channel_id=1, source_target_pairs={{8,12},{9,13},{10,14},{11,15},{24,28},{25,29},{26,30},{27,31}} | collective-permute-start | bytes 393224 | tf_op jit(solution)/shard_map/ppermute | solution.py:372
  41.1 9.9 %copy-start.8 = (bf16[2,128,512]{2,1,0:T(8,128)(2,1)}, bf16[2,128,512]{2,1,0:T(8,128)(2,1)S(1)}, u32[]{:S(2)}) copy-start(bf16[2,128,512]{2,1,0:T(8,128)(2,1)S(1)} %collective-permute-done.4.refs_8_) | copy-start | bytes 786436
  41.1 9.9 %collective-permute-start.6 = (bf16[1,128,512]{2,1,0:T(8,128)(2,1)S(1)}, bf16[1,128,512]{2,1,0:T(8,128)(2,1)S(1)}, u32[]{:S(2)}, u32[]{:S(2)}) collective-permute-start(bf16[1,128,512]{2,1,0:T(8,128)(2,1)S(1)} %slice.8), channel_id=1, source_target_pairs={{8,12},{9,13},{10,14},{11,15},{24,28},{25,29},{26,30},{27,31}} | collective-permute-start | bytes 393224 | tf_op jit(solution)/shard_map/ppermute | solution.py:372
  67.4 10.5 %collective-permute-start.8 = (bf16[512,512]{1,0:T(8,128)(2,1)}, bf16[512,512]{1,0:T(8,128)(2,1)S(1)}, u32[]{:S(2)}, u32[]{:S(2)}) collective-permute-start(bf16[512,512]{1,0:T(8,128)(2,1)} %bitcast.14), channel_id=1, source_target_pairs={{0,2},{1,3},{2,0},{3,1},{4,6},{5,7},{6,4},{7,5},{8,10},{9,11},{10,... | collective-permute-start | bytes 1572872 | tf_op jit(solution)/shard_map/ppermute | solution.py:421
  68.6 13.9 %collective-permute-start.10 = (bf16[512,512]{1,0:T(8,128)(2,1)}, bf16[512,512]{1,0:T(8,128)(2,1)S(1)}, u32[]{:S(2)}, u32[]{:S(2)}) collective-permute-start(bf16[512,512]{1,0:T(8,128)(2,1)} %bitcast.15), channel_id=1, source_target_pairs={{0,1},{1,0},{2,3},{3,2},{4,5},{5,4},{6,7},{7,6},{8,9},{9,8},{10,11... | collective-permute-start | bytes 1572872 | tf_op jit(solution)/shard_map/ppermute | solution.py:421
  77.8 10.6 %copy-start = (bf16[512,512]{1,0:T(8,128)(2,1)}, bf16[512,512]{1,0:T(8,128)(2,1)S(1)}, u32[]{:S(2)}) copy-start(bf16[512,512]{1,0:T(8,128)(2,1)S(1)} %collective-permute-done.8.a_ref) | copy-start | bytes 1572868
  77.8 10.6 %collective-permute-start.9 = (bf16[512,512]{1,0:T(8,128)(2,1)S(1)}, bf16[512,512]{1,0:T(8,128)(2,1)S(1)}, u32[]{:S(2)}, u32[]{:S(2)}) collective-permute-start(bf16[512,512]{1,0:T(8,128)(2,1)S(1)} %collective-permute-done.8.a_ref), channel_id=1, source_target_pairs={{0,1},{1,0},{2,3},{3,2},{4,5},{5,4},{6,7},{7,6},{8,9},{9,8},{10,11... | collective-permute-start | bytes 1572872 | tf_op jit(solution)/shard_map/ppermute | solution.py:421
  94.8 2.1 %collective-permute-start.11 = (bf16[4,32,1024]{2,1,0:T(8,128)(2,1)}, bf16[4,32,1024]{2,1,0:T(8,128)(2,1)S(1)}, u32[]{:S(2)}, u32[]{:S(2)}) collective-permute-start(bf16[4,32,1024]{2,1,0:T(8,128)(2,1)} %get-tuple-element.24), channel_id=1, source_target_pairs={{0,1},{1,0},{2,3},{3,2},{4,5},{5,4},{6,7},{7,6},{8,9},{9,8},{10,11... | collective-permute-start | bytes 786440 | tf_op jit(solution)/shard_map/ppermute | solution.py:421
  94.9 7.7 %collective-permute-start.12 = (bf16[4,32,1024]{2,1,0:T(8,128)(2,1)}, bf16[4,32,1024]{2,1,0:T(8,128)(2,1)S(1)}, u32[]{:S(2)}, u32[]{:S(2)}) collective-permute-start(bf16[4,32,1024]{2,1,0:T(8,128)(2,1)} %get-tuple-element.25), channel_id=1, source_target_pairs={{0,2},{1,3},{2,0},{3,1},{4,6},{5,7},{6,4},{7,5},{8,10},{9,11},{10,... | collective-permute-start | bytes 786440 | tf_op jit(solution)/shard_map/ppermute | solution.py:421
  96.1 12.6 %collective-permute-start.13 = (bf16[4,32,1024]{2,1,0:T(8,128)(2,1)}, bf16[4,32,1024]{2,1,0:T(8,128)(2,1)S(1)}, u32[]{:S(2)}, u32[]{:S(2)}) collective-permute-start(bf16[4,32,1024]{2,1,0:T(8,128)(2,1)} %get-tuple-element.26), channel_id=1, source_target_pairs={{0,3},{1,2},{2,1},{3,0},{4,7},{5,6},{6,5},{7,4},{8,11},{9,10},{10,... | collective-permute-start | bytes 786440 | tf_op jit(solution)/shard_map/ppermute | solution.py:421
  96.9 11.8 %copy-start.3 = (bf16[4,32,1024]{2,1,0:T(8,128)(2,1)}, bf16[4,32,1024]{2,1,0:T(8,128)(2,1)S(1)}, u32[]{:S(2)}) copy-start(bf16[4,32,1024]{2,1,0:T(8,128)(2,1)S(1)} %collective-permute-done.11.refs_1_) | copy-start | bytes 786436
  102.6 6.2 %copy-start.4 = (bf16[4,32,1024]{2,1,0:T(8,128)(2,1)}, bf16[4,32,1024]{2,1,0:T(8,128)(2,1)S(1)}, u32[]{:S(2)}) copy-start(bf16[4,32,1024]{2,1,0:T(8,128)(2,1)S(1)} %collective-permute-done.12.refs_2_) | copy-start | bytes 786436
  (7 other events, 5.5 us)

commit v3 on v2

--- a/solution.py
+++ b/solution.py
@@ -223,7 +223,7 @@
 def attend_kernel(len_ref, pos_ref, q_ref, gate_ref, *refs):
     own = (refs[0:2], refs[2:4])
     got_a, got_b, got_c, got_d = refs[4:6], refs[6:8], refs[8:10], refs[10:12]
-    pool_ref, out_ref = refs[12:]
+    pool_ref, *out_refs = refs[12:]
     seq_count, row_count, width = q_ref.shape
     head_count = width // HD
     lens, ranks = length_ranks(len_ref, seq_count)
@@ -238,7 +238,7 @@
         grouped = rows.astype(jnp.float32).reshape(per_block, L_CMP, width)
         return (grouped * weight[None]).sum(1)
 
-    def one_sequence(r, length, pieces):
+    def one_sequence(r, length, pieces, out_ref, at_out):
         count = len(pieces)
         join = lambda rows: rows[0] if count == 1 else jnp.concatenate(rows, axis=0)
         key_rows = [k[at] for (k, v), at in pieces]
@@ -269,9 +269,9 @@
             pick_gate = gates[:, head_count + h : head_count + h + 1] / total
             outs.append(pool_gate * pool + pick_gate * picked)
         mixed = jnp.where(live, jnp.concatenate(outs, axis=1), 0.0)
-        out_ref[r] = mixed.astype(jnp.bfloat16)
-
-    def pair_of(base, sources):
+        out_ref[at_out] = mixed.astype(jnp.bfloat16)
+
+    def pair_of(base, sources, out_ref):
         def one(at, carry):
             r = base + at
             length = jnp.int32(0)
@@ -281,19 +281,19 @@
 
             @pl.when(jnp.logical_not(alive))
             def _():
-                out_ref[r] = jnp.zeros((row_count, width), jnp.bfloat16)
+                out_ref[at] = jnp.zeros((row_count, width), jnp.bfloat16)
 
             for count in range(1, len(sources) + 1):
                 @pl.when(alive & (block == count - 1))
                 def _():
-                    one_sequence(r, length, [(x, at if x[0].shape[0] > 1 else 0) for x in sources[:count]])
+                    one_sequence(r, length, [(x, at if x[0].shape[0] > 1 else 0) for x in sources[:count]], out_ref, at)
 
             return carry
 
         lax.fori_loop(0, own[0][0].shape[0], one, 0)
 
-    pair_of(0, [own[0], got_a, got_c, got_d])
-    pair_of(own[0][0].shape[0], [own[1], got_b])
+    pair_of(0, [own[0], got_a, got_c, got_d], out_refs[0])
+    pair_of(own[0][0].shape[0], [own[1], got_b], out_refs[1])
 
 
 def part_product(rows_ref, w_ref):
@@ -409,78 +409,90 @@
             num_scalar_prefetch=2,
             grid=(1,),
             in_specs=[whole(o.shape) for o in operands],
-            out_specs=whole(queries.shape),
+            out_specs=[whole((two,) + queries.shape[1:])] * 2,
         ),
-        out_shape=jax.ShapeDtypeStruct(queries.shape, bf16),
+        out_shape=[jax.ShapeDtypeStruct((two,) + queries.shape[1:], bf16)] * 2,
         compiler_params=params,
         cost_estimate=cost(width, 2 * model_width),
         name="attend",
     )(lengths, kv_at[None], *operands)
 
-    attended = attended.reshape(flat, width)
     swap = lambda x, bit: lax.ppermute(x, "tp", [(t, t ^ bit) for t in range(tp_size)])
-    far_a = swap(attended, 2)
-    near_b = swap(attended, 1)
-    far_b = swap(far_a, 1)
     order = jnp.stack([tp_at, tp_at ^ 1, tp_at ^ 2, tp_at ^ 3])
     col_width = w_out.shape[1]
+    col_step = col_width // 2
     weight = w_out.reshape(tp_size, width, col_width)
+    piece = row_count // tp_size
+    rows_half = two * row_count
 
     def weight_spec(k):
-        return pl.BlockSpec((1, width, col_width), lambda i, n: (n[k], 0, 0))
-
-    near = pl.pallas_call(
-        near_kernel,
-        grid_spec=pltpu.PrefetchScalarGridSpec(
-            num_scalar_prefetch=1,
-            grid=(1,),
-            in_specs=[whole((flat, width))] * 2 + [weight_spec(0), weight_spec(1)],
-            out_specs=whole((flat, col_width)),
-        ),
-        out_shape=jax.ShapeDtypeStruct((flat, col_width), jnp.float32),
-        compiler_params=params,
-        cost_estimate=cost(col_width, 2 * width),
-        name="near_heads",
-    )(order, attended, near_b, weight, weight)
-    piece = row_count // tp_size
-    parts = pl.pallas_call(
-        far_kernel,
-        grid_spec=pltpu.PrefetchScalarGridSpec(
-            num_scalar_prefetch=1,
-            grid=(1,),
-            in_specs=[whole((flat, width))] * 2 + [weight_spec(2), weight_spec(3), whole((flat, col_width))],
-            out_specs=[whole((seq_count, piece, col_width))] * tp_size,
-            scratch_shapes=[pltpu.VMEM((seq_count, row_count, col_width), bf16)],
-        ),
-        out_shape=[jax.ShapeDtypeStruct((seq_count, piece, col_width), bf16)] * tp_size,
-        compiler_params=params,
-        cost_estimate=cost(col_width, 2 * width),
-        name="far_heads",
-    )(order, far_a, far_b, weight, weight, near)
-    got = [parts[0]] + [swap(parts[k], k) for k in (2, 3, 1)]
-    got = [got[0], got[3], got[1], got[2]]
+        return pl.BlockSpec((1, width, col_step), lambda i, n: (n[k], 0, i))
+
+    row_specs = [whole((rows_half, width))] * 2
+    near_spec = pl.BlockSpec((rows_half, col_step), lambda i, n: (0, i))
+    part_spec = pl.BlockSpec((two, piece, col_step), lambda i, n: (0, 0, i))
+    attended = [x.reshape(rows_half, width) for x in attended]
+    far_a, received = [], []
+    for at in range(2):
+        far_a.append(swap(attended[at], 2))
+    for at in range(2):
+        near_b = swap(attended[at], 1)
+        near = pl.pallas_call(
+            near_kernel,
+            grid_spec=pltpu.PrefetchScalarGridSpec(
+                num_scalar_prefetch=1,
+                grid=(2,),
+                in_specs=row_specs + [weight_spec(0), weight_spec(1)],
+                out_specs=near_spec,
+            ),
+            out_shape=jax.ShapeDtypeStruct((rows_half, col_width), jnp.float32),
+            compiler_params=params,
+            cost_estimate=cost(col_width, width),
+            name="near_heads",
+        )(order, attended[at], near_b, weight, weight)
+        far_b = swap(far_a[at], 1)
+        parts = pl.pallas_call(
+            far_kernel,
+            grid_spec=pltpu.PrefetchScalarGridSpec(
+                num_scalar_prefetch=1,
+                grid=(2,),
+                in_specs=row_specs + [weight_spec(2), weight_spec(3), near_spec],
+                out_specs=[part_spec] * tp_size,
+                scratch_shapes=[pltpu.VMEM((two, row_count, col_step), bf16)],
+            ),
+            out_shape=[jax.ShapeDtypeStruct((two, piece, col_width), bf16)] * tp_size,
+            compiler_params=params,
+            cost_estimate=cost(col_width, width),
+            name="far_heads",
+        )(order, far_a[at], far_b, weight, weight, near)
+        got = {k: swap(parts[k], k) for k in (2, 3, 1)}
+        received += [parts[0], got[1], got[2], got[3]]
     return pl.pallas_call(
         place_kernel,
         grid_spec=pltpu.PrefetchScalarGridSpec(
             num_scalar_prefetch=2,
             grid=(1,),
-            in_specs=[whole((seq_count, piece, col_width))] * tp_size,
+            in_specs=[whole((two, piece, col_width))] * (2 * tp_size),
             out_specs=whole((piece, seq_count, tp_size * col_width)),
         ),
         out_shape=jax.ShapeDtypeStruct((piece, seq_count, tp_size * col_width), bf16),
         compiler_params=params,
         name="place",
-    )(lengths, order, *got)
+    )(lengths, order, *received)
 
 
 def place_kernel(len_ref, idx_ref, *refs):
     out_ref = refs[-1]
-    seq_count, _, col_width = refs[0].shape
+    count = (len(refs) - 1) // 2
+    two, _, col_width = refs[0].shape
+    seq_count = out_ref.shape[1]
     _, ranks = length_ranks(len_ref, seq_count)
-    for k, part in enumerate(refs[:-1]):
+    for k in range(count):
         start = pl.multiple_of(idx_ref[k] * col_width, col_width)
         for s in range(seq_count):
-            out_ref[:, s, pl.ds(start, col_width)] = part[ranks[s]]
+            upper = refs[k][jnp.minimum(ranks[s], two - 1)]
+            lower = refs[count + k][jnp.maximum(ranks[s] - two, 0)]
+            out_ref[:, s, pl.ds(start, col_width)] = jnp.where(ranks[s] < two, upper, lower)
 
 
 def body(tokens, lengths, chosen, *weights):

time: 113 us -> 116 us (1.027)
  waiting for transfers between devices: 24.5 us -> 13.2 us
  starting transfers between devices: 29 us -> 36.7 us
  Pallas kernels: 54.4 us -> 59.6 us
    ppermute x6 -> x12, waiting for transfers between devices: 17.6 us -> 6.34 us  [live_body(): lax.ppermute(x, 'tp', [(t, t ^ bit) for t in range(tp_size)])]
    ppermute x6 -> x12, starting transfers between devices: 11 us -> 18.7 us  [live_body(): lax.ppermute(x, 'tp', [(t, t ^ bit) for t in range(tp_size)])]
    pallas_call x1 -> x2, Pallas kernels: 5.55 us -> 8.21 us  [live_body(): pl.pallas_call(far_kernel, grid_spec=pltpu.PrefetchScalarGridSpec(num_sca...]
    pallas_call x1 -> x2, Pallas kernels: 5.14 us -> 7.51 us  [live_body(): pl.pallas_call(near_kernel, grid_spec=pltpu.PrefetchScalarGridSpec(num_sc...]
    unnamed x34 -> x50, local copies, waits for them, and re-layouts: 3.17 us -> 4.27 us
  transfers between devices with their start and end apart: 14 -> 20, of which waited for: 5 -> 5; matrix products, arithmetic and copies ran while one was open for 1% -> 1% of each run, Pallas kernels for 13% -> 21%
where the time goes in v3:
time: 116 us
  Pallas kernels  59.6 us (51%)
  starting transfers between devices  36.7 us (32%)
  waiting for transfers between devices  13.2 us (11%)
  local copies, waits for them, and re-layouts  5.36 us (5%)
    ppermute x12, starting transfers between devices, live_body(): lax.ppermute(x, 'tp', [(t, t ^ bit) for t in range(tp_size)])  18.7 us
    ppermute x8, starting transfers between devices, live_body(): up = lambda x, pairs: lax.ppermute(x, 'kv', pairs)  18 us
    pallas_call x1, Pallas kernels, live_body(): pl.pallas_call(attend_kernel, grid_spec=pltpu.PrefetchScalarGridSpec(num_...  15.5 us
    pallas_call x1, Pallas kernels, live_body(): pl.pallas_call(q_kernel, grid_spec=pltpu.PrefetchScalarGridSpec(num_scala...  8.96 us
    pallas_call x1, Pallas kernels, live_body(): pl.pallas_call(first_kernel, grid_spec=pltpu.PrefetchScalarGridSpec(num_s...  8.85 us
    pallas_call x2, Pallas kernels, live_body(): pl.pallas_call(far_kernel, grid_spec=pltpu.PrefetchScalarGridSpec(num_sca...  8.21 us
    pallas_call x2, Pallas kernels, live_body(): pl.pallas_call(near_kernel, grid_spec=pltpu.PrefetchScalarGridSpec(num_sc...  7.51 us
    pallas_call x1, Pallas kernels, next_rows(): pl.pallas_call(next_kernel, grid_spec=pltpu.PrefetchScalarGridSpec(num_sc...  6.97 us
  transfers between devices with their start and end apart: 20, of which 5 were waited for; matrix products, arithmetic and copies ran while one was open for 1% of the time, Pallas kernels for 21%

profile of v3, /device:TPU:1, one launch (start us, length us, event | category | flops | bytes accessed | tf_op | source)
XLA Modules:
  0.0 115.9 jit_solution(4509985555325390128)
XLA Ops:
  0.0 8.9 %key_rows.1 = (bf16[2,128,512]{2,1,0:T(8,128)(2,1)}, bf16[2,128,512]{2,1,0:T(8,128)(2,1)}, bf16[32,512,128]{2,1,0:T(8,128)(2,1)}) custom-call(s32[4]{0:T(128)} %len_ref.9, bf16[128,4,4096]{2,1,0:T(4,128)(2,1)} %x_ref.1, bf16[4096,512]{1,0:T(8,128)(2,1)} %w_ref.2), custom_call_target="tpu_custom_call" | custom-call | flops 2147483648 | bytes 4194304 | tf_op jit(solution)/shard_map/key_rows/pallas_call | solution.py:339
  8.9 7.0 %value_rows.1 = (bf16[2,128,512]{2,1,0:T(8,128)(2,1)}, bf16[2,128,512]{2,1,0:T(8,128)(2,1)}) custom-call(s32[4]{0:T(128)} %len_ref.9, bf16[32,512,128]{2,1,0:T(8,128)(2,1)} %get-tuple-element.22.rows_ref, bf16[4096,512]{1,0:T(8,128)(2,1)} %w_ref.3), custom_call_target="tpu_custom_call" | custom-call | flops 2147483648 | bytes 4194304 | tf_op jit(solution)/shard_map/value_rows/pallas_call | solution.py:355
  15.8 4.0 %collective-permute-start.1 = (bf16[2,128,512]{2,1,0:T(8,128)(2,1)}, bf16[2,128,512]{2,1,0:T(8,128)(2,1)S(1)}, u32[]{:S(2)}, u32[]{:S(2)}) collective-permute-start(bf16[2,128,512]{2,1,0:T(8,128)(2,1)} %get-tuple-element.26.refs_1_), channel_id=1, source_target_pairs={{0,4},{4,8},{8,12},{1,5},{5,9},{9,13},{2,6},{6,10},{10,14},{3,7},{... | collective-permute-start | bytes 786440 | tf_op jit(solution)/shard_map/ppermute | solution.py:372
  19.9 3.2 %collective-permute-start = (bf16[2,128,512]{2,1,0:T(8,128)(2,1)S(1)}, bf16[2,128,512]{2,1,0:T(8,128)(2,1)S(1)}, u32[]{:S(2)}, u32[]{:S(2)}) collective-permute-start(bf16[2,128,512]{2,1,0:T(8,128)(2,1)S(1)} %copy-done.15), channel_id=1, source_target_pairs={{0,4},{4,8},{8,12},{1,5},{5,9},{9,13},{2,6},{6,10},{10,14},{3,7},{... | collective-permute-start | bytes 786440 | tf_op jit(solution)/shard_map/ppermute | solution.py:372
  23.1 2.0 %collective-permute-done.1.refs_5_ = bf16[2,128,512]{2,1,0:T(8,128)(2,1)S(1)} collective-permute-done((bf16[2,128,512]{2,1,0:T(8,128)(2,1)}, bf16[2,128,512]{2,1,0:T(8,128)(2,1)S(1)}, u32[]{:S(2)}, u32[]{:S(2)}) %collective-permute-start.1) | collective-permute-done | bytes 262176 | tf_op jit(solution)/shard_map/ppermute | solution.py:372
  25.8 4.8 %collective-permute-done.refs_4_ = bf16[2,128,512]{2,1,0:T(8,128)(2,1)S(1)} collective-permute-done((bf16[2,128,512]{2,1,0:T(8,128)(2,1)S(1)}, bf16[2,128,512]{2,1,0:T(8,128)(2,1)S(1)}, u32[]{:S(2)}, u32[]{:S(2)}) %collective-permute-start) | collective-permute-done | bytes 262176 | tf_op jit(solution)/shard_map/ppermute | solution.py:372
  31.3 6.7 %collective-permute-start.3 = (bf16[2,128,512]{2,1,0:T(8,128)(2,1)}, bf16[2,128,512]{2,1,0:T(8,128)(2,1)S(1)}, u32[]{:S(2)}, u32[]{:S(2)}) collective-permute-start(bf16[2,128,512]{2,1,0:T(8,128)(2,1)} %get-tuple-element.28.refs_3_), channel_id=1, source_target_pairs={{0,4},{1,5},{2,6},{3,7},{16,20},{17,21},{18,22},{19,23}} | collective-permute-start | bytes 786440 | tf_op jit(solution)/shard_map/ppermute | solution.py:372
  38.0 1.3 %collective-permute-start.2 = (bf16[2,128,512]{2,1,0:T(8,128)(2,1)S(1)}, bf16[2,128,512]{2,1,0:T(8,128)(2,1)S(1)}, u32[]{:S(2)}, u32[]{:S(2)}) collective-permute-start(bf16[2,128,512]{2,1,0:T(8,128)(2,1)S(1)} %copy-done.16), channel_id=1, source_target_pairs={{0,4},{1,5},{2,6},{3,7},{16,20},{17,21},{18,22},{19,23}} | collective-permute-start | bytes 786440 | tf_op jit(solution)/shard_map/ppermute | solution.py:372
  39.3 1.1 pad.4.wg_ref
  42.0 9.0 %query_rows.1 = (bf16[4,128,512]{2,1,0:T(8,128)(2,1)}, f32[4,128,128]{2,1,0:T(8,128)}) custom-call(s32[4]{0:T(128)} %len_ref.9, bf16[32,512,128]{2,1,0:T(8,128)(2,1)} %get-tuple-element.22.rows_ref, bf16[4096,512]{1,0:T(8,128)(2,1)} %wq_ref.1, bf16[128,4096]{1,0:T(8,128)(2,1)} %pad.4.wg_ref), custom_call_target="tpu_custom_call" | custom-call | flops 2684354560 | bytes 5242880 | tf_op jit(solution)/shard_map/query_rows/pallas_call | solution.py:384
  51.9 15.5 %attend.1 = (bf16[2,128,512]{2,1,0:T(8,128)(2,1)}, bf16[2,128,512]{2,1,0:T(8,128)(2,1)}) custom-call(s32[4]{0:T(128)} %len_ref.9, s32[1]{0:T(128)} %bitcast.4.pos_ref, bf16[4,128,512]{2,1,0:T(8,128)(2,1)} %get-tuple-element.23.q_ref, f32[4,128,128]{2,1,0:T(8,128)} %get-tuple-element.24.gate_ref, bf16[2,128,512]{2,1,0:T(8,128)(2,1)} %get-tuple-element.25.refs_0_, ...), custom_call_target="tpu_custom_call" | custom-call | flops 4294967296 | bytes 8388608 | tf_op jit(solution)/shard_map/attend/pallas_call | solution.py:406
  67.3 1.2 %collective-permute-start.8 = (bf16[256,512]{1,0:T(8,128)(2,1)}, bf16[256,512]{1,0:T(8,128)(2,1)S(1)}, u32[]{:S(2)}, u32[]{:S(2)}) collective-permute-start(bf16[256,512]{1,0:T(8,128)(2,1)} %bitcast.22), channel_id=1, source_target_pairs={{0,2},{1,3},{2,0},{3,1},{4,6},{5,7},{6,4},{7,5},{8,10},{9,11},{10,... | collective-permute-start | bytes 786440 | tf_op jit(solution)/shard_map/ppermute | solution.py:420
  68.8 3.8 %collective-permute-start.10 = (bf16[256,512]{1,0:T(8,128)(2,1)}, bf16[256,512]{1,0:T(8,128)(2,1)S(1)}, u32[]{:S(2)}, u32[]{:S(2)}) collective-permute-start(bf16[256,512]{1,0:T(8,128)(2,1)} %bitcast.23), channel_id=1, source_target_pairs={{0,1},{1,0},{2,3},{3,2},{4,5},{5,4},{6,7},{7,6},{8,9},{9,8},{10,11... | collective-permute-start | bytes 786440 | tf_op jit(solution)/shard_map/ppermute | solution.py:420
  72.8 6.3 %collective-permute-start.9 = (bf16[256,512]{1,0:T(8,128)(2,1)S(1)}, bf16[256,512]{1,0:T(8,128)(2,1)S(1)}, u32[]{:S(2)}, u32[]{:S(2)}) collective-permute-start(bf16[256,512]{1,0:T(8,128)(2,1)S(1)} %collective-permute-done.8.a_ref), channel_id=1, source_target_pairs={{0,1},{1,0},{2,3},{3,2},{4,5},{5,4},{6,7},{7,6},{8,9},{9,8},{10,11... | collective-permute-start | bytes 786440 | tf_op jit(solution)/shard_map/ppermute | solution.py:420
  79.1 2.8 %collective-permute-start.15 = (bf16[256,512]{1,0:T(8,128)(2,1)S(1)}, bf16[256,512]{1,0:T(8,128)(2,1)S(1)}, u32[]{:S(2)}, u32[]{:S(2)}) collective-permute-start(bf16[256,512]{1,0:T(8,128)(2,1)S(1)} %collective-permute-done.14.a_ref), channel_id=1, source_target_pairs={{0,1},{1,0},{2,3},{3,2},{4,5},{5,4},{6,7},{7,6},{8,9},{9,8},{10,11... | collective-permute-start | bytes 786440 | tf_op jit(solution)/shard_map/ppermute | solution.py:420
  83.2 3.8 %near_heads.2.near_ref = f32[256,1024]{1,0:T(8,128)} custom-call(s32[4]{0:T(128)} %pad_add_fusion.idx_ref, bf16[256,512]{1,0:T(8,128)(2,1)} %bitcast.24, bf16[256,512]{1,0:T(8,128)(2,1)} %copy-done.5, bf16[4,512,1024]{2,1,0:T(8,128)(2,1)} %bitcast.11, bf16[4,512,1024]{2,1,0:T(8,128)(2,1)} %bitcast.12), custom_call_target="tpu_custom_call" | custom-call | flops 536870912 | bytes 1048576 | tf_op jit(solution)/shard_map/near_heads/pallas_call | solution.py:440
  87.7 4.1 %far_heads.2 = (bf16[2,32,1024]{2,1,0:T(8,128)(2,1)}, bf16[2,32,1024]{2,1,0:T(8,128)(2,1)}, bf16[2,32,1024]{2,1,0:T(8,128)(2,1)}, bf16[2,32,1024]{2,1,0:T(8,128)(2,1)}) custom-call(s32[4]{0:T(128)} %pad_add_fusion.idx_ref, bf16[256,512]{1,0:T(8,128)(2,1)} %copy-done.1, bf16[256,512]{1,0:T(8,128)(2,1)} %copy-done.4, bf16[4,512,1024]{2,1,0:T(8,128)(2,1)} %bitcast.13, ...), custom_call_target="tpu_custom_call" | custom-call | flops 536870912 | bytes 1048576 | tf_op jit(solution)/shard_map/far_heads/pallas_call | solution.py:454
  92.5 3.8 %near_heads.3.near_ref = f32[256,1024]{1,0:T(8,128)} custom-call(s32[4]{0:T(128)} %pad_add_fusion.idx_ref, bf16[256,512]{1,0:T(8,128)(2,1)} %bitcast.21, bf16[256,512]{1,0:T(8,128)(2,1)} %copy-done.2, bf16[4,512,1024]{2,1,0:T(8,128)(2,1)} %bitcast.15, bf16[4,512,1024]{2,1,0:T(8,128)(2,1)} %bitcast.16), custom_call_target="tpu_custom_call" | custom-call | flops 536870912 | bytes 1048576 | tf_op jit(solution)/shard_map/near_heads/pallas_call | solution.py:440
  96.3 1.2 %collective-permute-start.12 = (bf16[2,32,1024]{2,1,0:T(8,128)(2,1)S(1)}, bf16[2,32,1024]{2,1,0:T(8,128)(2,1)S(1)}, u32[]{:S(2)}, u32[]{:S(2)}) collective-permute-start(bf16[2,32,1024]{2,1,0:T(8,128)(2,1)S(1)} %copy-done.22), channel_id=1, source_target_pairs={{0,2},{1,3},{2,0},{3,1},{4,6},{5,7},{6,4},{7,5},{8,10},{9,11},{10,... | collective-permute-start | bytes 393224 | tf_op jit(solution)/shard_map/ppermute | solution.py:420
  99.1 4.1 %far_heads.3 = (bf16[2,32,1024]{2,1,0:T(8,128)(2,1)}, bf16[2,32,1024]{2,1,0:T(8,128)(2,1)}, bf16[2,32,1024]{2,1,0:T(8,128)(2,1)}, bf16[2,32,1024]{2,1,0:T(8,128)(2,1)}) custom-call(s32[4]{0:T(128)} %pad_add_fusion.idx_ref, bf16[256,512]{1,0:T(8,128)(2,1)} %copy-done, bf16[256,512]{1,0:T(8,128)(2,1)} %copy-done.3, bf16[4,512,1024]{2,1,0:T(8,128)(2,1)} %bitcast.17, ...), custom_call_target="tpu_custom_call" | custom-call | flops 536870912 | bytes 1048576 | tf_op jit(solution)/shard_map/far_heads/pallas_call | solution.py:454
  103.3 1.3 %collective-permute-start.18 = (bf16[2,32,1024]{2,1,0:T(8,128)(2,1)}, bf16[2,32,1024]{2,1,0:T(8,128)(2,1)S(1)}, u32[]{:S(2)}, u32[]{:S(2)}) collective-permute-start(bf16[2,32,1024]{2,1,0:T(8,128)(2,1)} %get-tuple-element.37), channel_id=1, source_target_pairs={{0,2},{1,3},{2,0},{3,1},{4,6},{5,7},{6,4},{7,5},{8,10},{9,11},{10,... | collective-permute-start | bytes 393224 | tf_op jit(solution)/shard_map/ppermute | solution.py:420
  105.4 2.7 %collective-permute-done.18.refs_6_ = bf16[2,32,1024]{2,1,0:T(8,128)(2,1)S(1)} collective-permute-done((bf16[2,32,1024]{2,1,0:T(8,128)(2,1)}, bf16[2,32,1024]{2,1,0:T(8,128)(2,1)S(1)}, u32[]{:S(2)}, u32[]{:S(2)}) %collective-permute-start.18) | collective-permute-done | bytes 131104 | tf_op jit(solution)/shard_map/ppermute | solution.py:420
  108.2 3.4 %collective-permute-done.19.refs_7_ = bf16[2,32,1024]{2,1,0:T(8,128)(2,1)S(1)} collective-permute-done((bf16[2,32,1024]{2,1,0:T(8,128)(2,1)}, bf16[2,32,1024]{2,1,0:T(8,128)(2,1)S(1)}, u32[]{:S(2)}, u32[]{:S(2)}) %collective-permute-start.19) | collective-permute-done | bytes 131104 | tf_op jit(solution)/shard_map/ppermute | solution.py:420
  112.2 3.6 %place.1 = bf16[32,4,4096]{2,1,0:T(4,128)(2,1)} custom-call(s32[4]{0:T(128)} %len_ref.9, s32[4]{0:T(128)} %pad_add_fusion.idx_ref, bf16[2,32,1024]{2,1,0:T(8,128)(2,1)} %get-tuple-element.30.refs_0_, bf16[2,32,1024]{2,1,0:T(8,128)(2,1)} %copy-done.7, bf16[2,32,1024]{2,1,0:T(8,128)(2,1)} %copy-done.8, bf16[2,32,1024]{2,1,0:T(8,128)(2,1)} %copy-done.9, ...), custom_call_target="tpu_custom_call" | custom-call | tf_op jit(solution)/shard_map/place/pallas_call | solution.py:470
  (79 shorter events, 10.1 us)
Async XLA Ops:
  8.9 29.1 %copy-start.16 = (bf16[2,128,512]{2,1,0:T(8,128)(2,1)S(1)}, bf16[2,128,512]{2,1,0:T(8,128)(2,1)}, u32[]{:S(2)}) copy-start(bf16[2,128,512]{2,1,0:T(8,128)(2,1)} %get-tuple-element.27.refs_2_) | copy-start | bytes 786436
  8.9 30.5 %copy-start.6 = (bf16[4096,2,8]{0,2,1:T(8,128)(2,1)S(1)}, bf16[4096,2,8]{0,2,1:T(8,128)(2,1)}, u32[]{:S(2)}) copy-start(bf16[4096,2,8]{0,2,1:T(8,128)(2,1)} %param.14) | copy-start | bytes 393220
  15.8 9.3 %collective-permute-start.1 = (bf16[2,128,512]{2,1,0:T(8,128)(2,1)}, bf16[2,128,512]{2,1,0:T(8,128)(2,1)S(1)}, u32[]{:S(2)}, u32[]{:S(2)}) collective-permute-start(bf16[2,128,512]{2,1,0:T(8,128)(2,1)} %get-tuple-element.26.refs_1_), channel_id=1, source_target_pairs={{0,4},{4,8},{8,12},{1,5},{5,9},{9,13},{2,6},{6,10},{10,14},{3,7},{... | collective-permute-start | bytes 786440 | tf_op jit(solution)/shard_map/ppermute | solution.py:372
  19.9 10.8 %collective-permute-start = (bf16[2,128,512]{2,1,0:T(8,128)(2,1)S(1)}, bf16[2,128,512]{2,1,0:T(8,128)(2,1)S(1)}, u32[]{:S(2)}, u32[]{:S(2)}) collective-permute-start(bf16[2,128,512]{2,1,0:T(8,128)(2,1)S(1)} %copy-done.15), channel_id=1, source_target_pairs={{0,4},{4,8},{8,12},{1,5},{5,9},{9,13},{2,6},{6,10},{10,14},{3,7},{... | collective-permute-start | bytes 786440 | tf_op jit(solution)/shard_map/ppermute | solution.py:372
  25.1 25.8 %copy-start.17 = (bf16[2,128,512]{2,1,0:T(8,128)(2,1)}, bf16[2,128,512]{2,1,0:T(8,128)(2,1)S(1)}, u32[]{:S(2)}) copy-start(bf16[2,128,512]{2,1,0:T(8,128)(2,1)S(1)} %collective-permute-done.1.refs_5_) | copy-start | bytes 786436
  25.1 15.3 %collective-permute-start.5 = (bf16[2,128,512]{2,1,0:T(8,128)(2,1)S(1)}, bf16[2,128,512]{2,1,0:T(8,128)(2,1)S(1)}, u32[]{:S(2)}, u32[]{:S(2)}) collective-permute-start(bf16[2,128,512]{2,1,0:T(8,128)(2,1)S(1)} %collective-permute-done.1.refs_5_), channel_id=1, source_target_pairs={{4,8},{8,12},{5,9},{9,13},{6,10},{10,14},{7,11},{11,15},{20,24},{2... | collective-permute-start | bytes 786440 | tf_op jit(solution)/shard_map/ppermute | solution.py:372
  30.6 20.3 %copy-start.18 = (bf16[2,128,512]{2,1,0:T(8,128)(2,1)}, bf16[2,128,512]{2,1,0:T(8,128)(2,1)S(1)}, u32[]{:S(2)}) copy-start(bf16[2,128,512]{2,1,0:T(8,128)(2,1)S(1)} %collective-permute-done.refs_4_) | copy-start | bytes 786436
  30.6 10.5 %collective-permute-start.4 = (bf16[2,128,512]{2,1,0:T(8,128)(2,1)S(1)}, bf16[2,128,512]{2,1,0:T(8,128)(2,1)S(1)}, u32[]{:S(2)}, u32[]{:S(2)}) collective-permute-start(bf16[2,128,512]{2,1,0:T(8,128)(2,1)S(1)} %collective-permute-done.refs_4_), channel_id=1, source_target_pairs={{4,8},{8,12},{5,9},{9,13},{6,10},{10,14},{7,11},{11,15},{20,24},{2... | collective-permute-start | bytes 786440 | tf_op jit(solution)/shard_map/ppermute | solution.py:372
  31.3 19.7 %collective-permute-start.3 = (bf16[2,128,512]{2,1,0:T(8,128)(2,1)}, bf16[2,128,512]{2,1,0:T(8,128)(2,1)S(1)}, u32[]{:S(2)}, u32[]{:S(2)}) collective-permute-start(bf16[2,128,512]{2,1,0:T(8,128)(2,1)} %get-tuple-element.28.refs_3_), channel_id=1, source_target_pairs={{0,4},{1,5},{2,6},{3,7},{16,20},{17,21},{18,22},{19,23}} | collective-permute-start | bytes 786440 | tf_op jit(solution)/shard_map/ppermute | solution.py:372
  38.0 13.0 %collective-permute-start.2 = (bf16[2,128,512]{2,1,0:T(8,128)(2,1)S(1)}, bf16[2,128,512]{2,1,0:T(8,128)(2,1)S(1)}, u32[]{:S(2)}, u32[]{:S(2)}) collective-permute-start(bf16[2,128,512]{2,1,0:T(8,128)(2,1)S(1)} %copy-done.16), channel_id=1, source_target_pairs={{0,4},{1,5},{2,6},{3,7},{16,20},{17,21},{18,22},{19,23}} | collective-permute-start | bytes 786440 | tf_op jit(solution)/shard_map/ppermute | solution.py:372
  40.4 10.6 %collective-permute-start.7 = (bf16[1,128,512]{2,1,0:T(8,128)(2,1)S(1)}, bf16[1,128,512]{2,1,0:T(8,128)(2,1)S(1)}, u32[]{:S(2)}, u32[]{:S(2)}) collective-permute-start(bf16[1,128,512]{2,1,0:T(8,128)(2,1)S(1)} %slice.9), channel_id=1, source_target_pairs={{8,12},{9,13},{10,14},{11,15},{24,28},{25,29},{26,30},{27,31}} | collective-permute-start | bytes 393224 | tf_op jit(solution)/shard_map/ppermute | solution.py:372
  41.1 9.9 %collective-permute-start.6 = (bf16[1,128,512]{2,1,0:T(8,128)(2,1)S(1)}, bf16[1,128,512]{2,1,0:T(8,128)(2,1)S(1)}, u32[]{:S(2)}, u32[]{:S(2)}) collective-permute-start(bf16[1,128,512]{2,1,0:T(8,128)(2,1)S(1)} %slice.8), channel_id=1, source_target_pairs={{8,12},{9,13},{10,14},{11,15},{24,28},{25,29},{26,30},{27,31}} | collective-permute-start | bytes 393224 | tf_op jit(solution)/shard_map/ppermute | solution.py:372
  67.3 5.4 %collective-permute-start.8 = (bf16[256,512]{1,0:T(8,128)(2,1)}, bf16[256,512]{1,0:T(8,128)(2,1)S(1)}, u32[]{:S(2)}, u32[]{:S(2)}) collective-permute-start(bf16[256,512]{1,0:T(8,128)(2,1)} %bitcast.22), channel_id=1, source_target_pairs={{0,2},{1,3},{2,0},{3,1},{4,6},{5,7},{6,4},{7,5},{8,10},{9,11},{10,... | collective-permute-start | bytes 786440 | tf_op jit(solution)/shard_map/ppermute | solution.py:420
  68.6 10.5 %collective-permute-start.14 = (bf16[256,512]{1,0:T(8,128)(2,1)}, bf16[256,512]{1,0:T(8,128)(2,1)S(1)}, u32[]{:S(2)}, u32[]{:S(2)}) collective-permute-start(bf16[256,512]{1,0:T(8,128)(2,1)} %bitcast.19), channel_id=1, source_target_pairs={{0,2},{1,3},{2,0},{3,1},{4,6},{5,7},{6,4},{7,5},{8,10},{9,11},{10,... | collective-permute-start | bytes 786440 | tf_op jit(solution)/shard_map/ppermute | solution.py:420
  68.8 13.7 %collective-permute-start.10 = (bf16[256,512]{1,0:T(8,128)(2,1)}, bf16[256,512]{1,0:T(8,128)(2,1)S(1)}, u32[]{:S(2)}, u32[]{:S(2)}) collective-permute-start(bf16[256,512]{1,0:T(8,128)(2,1)} %bitcast.23), channel_id=1, source_target_pairs={{0,1},{1,0},{2,3},{3,2},{4,5},{5,4},{6,7},{7,6},{8,9},{9,8},{10,11... | collective-permute-start | bytes 786440 | tf_op jit(solution)/shard_map/ppermute | solution.py:420
  72.8 14.2 %collective-permute-start.9 = (bf16[256,512]{1,0:T(8,128)(2,1)S(1)}, bf16[256,512]{1,0:T(8,128)(2,1)S(1)}, u32[]{:S(2)}, u32[]{:S(2)}) collective-permute-start(bf16[256,512]{1,0:T(8,128)(2,1)S(1)} %collective-permute-done.8.a_ref), channel_id=1, source_target_pairs={{0,1},{1,0},{2,3},{3,2},{4,5},{5,4},{6,7},{7,6},{8,9},{9,8},{10,11... | collective-permute-start | bytes 786440 | tf_op jit(solution)/shard_map/ppermute | solution.py:420
  79.1 12.7 %collective-permute-start.16 = (bf16[256,512]{1,0:T(8,128)(2,1)}, bf16[256,512]{1,0:T(8,128)(2,1)S(1)}, u32[]{:S(2)}, u32[]{:S(2)}) collective-permute-start(bf16[256,512]{1,0:T(8,128)(2,1)} %bitcast.20), channel_id=1, source_target_pairs={{0,1},{1,0},{2,3},{3,2},{4,5},{5,4},{6,7},{7,6},{8,9},{9,8},{10,11... | collective-permute-start | bytes 786440 | tf_op jit(solution)/shard_map/ppermute | solution.py:420
  79.1 19.3 %collective-permute-start.15 = (bf16[256,512]{1,0:T(8,128)(2,1)S(1)}, bf16[256,512]{1,0:T(8,128)(2,1)S(1)}, u32[]{:S(2)}, u32[]{:S(2)}) collective-permute-start(bf16[256,512]{1,0:T(8,128)(2,1)S(1)} %collective-permute-done.14.a_ref), channel_id=1, source_target_pairs={{0,1},{1,0},{2,3},{3,2},{4,5},{5,4},{6,7},{7,6},{8,9},{9,8},{10,11... | collective-permute-start | bytes 786440 | tf_op jit(solution)/shard_map/ppermute | solution.py:420
  91.7 12.8 %collective-permute-start.11 = (bf16[2,32,1024]{2,1,0:T(8,128)(2,1)}, bf16[2,32,1024]{2,1,0:T(8,128)(2,1)S(1)}, u32[]{:S(2)}, u32[]{:S(2)}) collective-permute-start(bf16[2,32,1024]{2,1,0:T(8,128)(2,1)} %get-tuple-element.31), channel_id=1, source_target_pairs={{0,1},{1,0},{2,3},{3,2},{4,5},{5,4},{6,7},{7,6},{8,9},{9,8},{10,11... | collective-permute-start | bytes 393224 | tf_op jit(solution)/shard_map/ppermute | solution.py:420
  96.3 9.1 %collective-permute-start.12 = (bf16[2,32,1024]{2,1,0:T(8,128)(2,1)S(1)}, bf16[2,32,1024]{2,1,0:T(8,128)(2,1)S(1)}, u32[]{:S(2)}, u32[]{:S(2)}) collective-permute-start(bf16[2,32,1024]{2,1,0:T(8,128)(2,1)S(1)} %copy-done.22), channel_id=1, source_target_pairs={{0,2},{1,3},{2,0},{3,1},{4,6},{5,7},{6,4},{7,5},{8,10},{9,11},{10,... | collective-permute-start | bytes 393224 | tf_op jit(solution)/shard_map/ppermute | solution.py:420
  97.5 7.9 %collective-permute-start.13 = (bf16[2,32,1024]{2,1,0:T(8,128)(2,1)S(1)}, bf16[2,32,1024]{2,1,0:T(8,128)(2,1)S(1)}, u32[]{:S(2)}, u32[]{:S(2)}) collective-permute-start(bf16[2,32,1024]{2,1,0:T(8,128)(2,1)S(1)} %copy-done.21), channel_id=1, source_target_pairs={{0,3},{1,2},{2,1},{3,0},{4,7},{5,6},{6,5},{7,4},{8,11},{9,10},{10,... | collective-permute-start | bytes 393224 | tf_op jit(solution)/shard_map/ppermute | solution.py:420
  103.3 2.2 %collective-permute-start.17 = (bf16[2,32,1024]{2,1,0:T(8,128)(2,1)}, bf16[2,32,1024]{2,1,0:T(8,128)(2,1)S(1)}, u32[]{:S(2)}, u32[]{:S(2)}) collective-permute-start(bf16[2,32,1024]{2,1,0:T(8,128)(2,1)} %get-tuple-element.36), channel_id=1, source_target_pairs={{0,1},{1,0},{2,3},{3,2},{4,5},{5,4},{6,7},{7,6},{8,9},{9,8},{10,11... | collective-permute-start | bytes 393224 | tf_op jit(solution)/shard_map/ppermute | solution.py:420
  103.3 4.9 %collective-permute-start.18 = (bf16[2,32,1024]{2,1,0:T(8,128)(2,1)}, bf16[2,32,1024]{2,1,0:T(8,128)(2,1)S(1)}, u32[]{:S(2)}, u32[]{:S(2)}) collective-permute-start(bf16[2,32,1024]{2,1,0:T(8,128)(2,1)} %get-tuple-element.37), channel_id=1, source_target_pairs={{0,2},{1,3},{2,0},{3,1},{4,6},{5,7},{6,4},{7,5},{8,10},{9,11},{10,... | collective-permute-start | bytes 393224 | tf_op jit(solution)/shard_map/ppermute | solution.py:420
  104.5 7.0 %collective-permute-start.19 = (bf16[2,32,1024]{2,1,0:T(8,128)(2,1)}, bf16[2,32,1024]{2,1,0:T(8,128)(2,1)S(1)}, u32[]{:S(2)}, u32[]{:S(2)}) collective-permute-start(bf16[2,32,1024]{2,1,0:T(8,128)(2,1)} %get-tuple-element.38), channel_id=1, source_target_pairs={{0,3},{1,2},{2,1},{3,0},{4,7},{5,6},{6,5},{7,4},{8,11},{9,10},{10,... | collective-permute-start | bytes 393224 | tf_op jit(solution)/shard_map/ppermute | solution.py:420
  (21 other events, 99.3 us)
